TPU v7x, 32 devices: a whole 2x2x4 slice. The times are simulated.
32 devices in a mesh: gr: 2 (over x), fs: 8 (over z, y), tp: 2 (over core).
Axes of the slice: x: 2, y: 2, z: 4, core: 2. Of those that a mesh axis runs over, the one named last changes fastest.
Arguments:
- tokens: bfloat16 [4096, 2048], P(('gr', 'fs')), may hold values from -6 to 6
- norm_gain: float32 [2048], P(('gr', 'fs')), may hold values from 0.1 to 1.9
- gate_train: float32 [8, 2048, 1024], P(None, ('gr', 'fs'), 'tp'), may hold values from -0.125 to 0.125
- up_train: float32 [8, 2048, 1024], P(None, ('gr', 'fs'), 'tp'), may hold values from -0.125 to 0.125
- down_train: float32 [8, 1024, 2048], P(None, 'tp', ('gr', 'fs')), may hold values from -0.1875 to 0.1875
- expert_ids: int32 [4096, 2], P(('gr', 'fs')), may hold values from 0 to 7, all different within a row; in each aligned block of 256 rows (0 to 255, 256 to 511, ...) at most 128 rows name the same one
- route_score: float32 [4096, 2], P(('gr', 'fs')), may hold values from 0.05 to 1
Outputs:
- gate_ready: bfloat16 [8, 2048, 1024], P('fs', None, 'tp')
- up_ready: bfloat16 [8, 2048, 1024], P('fs', None, 'tp')
- down_ready: bfloat16 [8, 1024, 2048], P('fs', 'tp')
- mixed: bfloat16 [4096, 2048], P(('gr', 'fs'), 'tp')
Inputs may be any that keep to these rules, and one draw needn't show every extreme that they name: `expert_ids`: each row names two different experts. Among the 256 rows of one device no expert is named more than 128 times, and in every draw some expert is named exactly 128 times by some device's rows.
All inputs are finite; a program needn't handle non-finite values.
Results may differ from a plain program's by a relative error of at most 0.015.
Values may be sent and summed in bfloat16 or wider, within the bound.
No kernel may reach another device: no remote copies, remote signals or barrier semaphores. Data moves between devices by JAX's collectives and lax.ppermute only.
A program may use at most 64 MiB of HBM per device.

v0:
```python
import jax
import jax.numpy as jnp
from jax import lax
from jax.sharding import PartitionSpec as P

epsilon = 1e-06


def shortened(shard):
    return jax.tree.map(lambda a: a.astype(jnp.bfloat16) if a.dtype == jnp.float32 else a, shard)


def move_inputs(gate_cast, up_cast):
    spread = (
        lax.all_to_all(gate_cast[:, None], "fs", split_axis=0, concat_axis=1, tiled=True),
        lax.all_to_all(up_cast[:, None], "fs", split_axis=0, concat_axis=1, tiled=True),
    )
    flattened = tuple((piece.reshape(piece.shape[0], 1, -1, piece.shape[-1]) for piece in spread))
    owned = jax.tree.map(
        lambda part, own: part.astype(own.dtype),
        lax.all_gather(shortened(flattened), "gr", axis=1, tiled=True),
        flattened,
    )
    return tuple((piece.reshape(piece.shape[0], -1, piece.shape[-1]) for piece in owned))


def move_down(down_cast):
    spread = lax.all_to_all(down_cast[:, :, None], "fs", split_axis=0, concat_axis=2, tiled=True)
    flattened = spread.reshape(spread.shape[0], spread.shape[1], 1, -1)
    owned = lax.all_gather(flattened, "gr", axis=2, tiled=True)
    return owned.reshape(owned.shape[0], owned.shape[1], -1)


def on_device(tokens, norm_gain, gate_train, up_train, down_train, expert_ids, route_score):
    gate_cast = (norm_gain[None, :, None] * gate_train).astype(jnp.bfloat16)
    up_cast = (norm_gain[None, :, None] * up_train).astype(jnp.bfloat16)
    down_cast = down_train.astype(jnp.bfloat16)
    fs_count = lax.axis_size("fs")
    experts = gate_train.shape[0]
    tok_count = tokens.shape[0]
    width = tokens.shape[1]
    capacity = 4 * tok_count // experts
    gate_ready, up_ready = move_inputs(gate_cast, up_cast)
    down_ready = move_down(down_cast)
    floated = tokens.astype(jnp.float32)
    normed = (
        floated * lax.rsqrt(jnp.mean(floated * floated, axis=-1, keepdims=True) + epsilon)
    ).astype(jnp.bfloat16)
    flat_ids = expert_ids.reshape(-1)
    matches = (flat_ids[:, None] == jnp.arange(experts, dtype=jnp.int32)[None, :]).astype(jnp.int32)
    ranked = jnp.sum((jnp.cumsum(matches, axis=0) - 1) * matches, axis=1)
    slot_index = flat_ids * capacity + ranked
    pick_token = jnp.arange(flat_ids.shape[0], dtype=jnp.int32) // 2
    slot_token = jnp.zeros((experts * capacity,), jnp.int32).at[slot_index].set(pick_token)
    filled = jnp.zeros((experts * capacity,), jnp.bool_).at[slot_index].set(True)
    gathered_rows = jnp.where(filled[:, None], normed[slot_token], jnp.zeros((), jnp.bfloat16))
    outgoing = gathered_rows.reshape(fs_count, experts // fs_count, capacity, width)
    received = lax.all_to_all(outgoing, "fs", split_axis=0, concat_axis=0, tiled=True)
    gate_act = jnp.einsum(
        "seck,ekh->sech", received, gate_ready, preferred_element_type=jnp.float32
    )
    up_act = jnp.einsum("seck,ekh->sech", received, up_ready, preferred_element_type=jnp.float32)
    hidden = (jax.nn.silu(gate_act) * up_act).astype(jnp.bfloat16)
    partial_value = jnp.einsum(
        "sech,ehk->seck", hidden, down_ready, preferred_element_type=jnp.float32
    )
    summed = lax.psum_scatter(
        partial_value.astype(jnp.bfloat16), "tp", scatter_dimension=3, tiled=True
    )
    returned = lax.all_to_all(summed, "fs", split_axis=0, concat_axis=0, tiled=True)
    flat_back = returned.reshape(experts * capacity, -1)
    picked = flat_back[slot_index].reshape(tok_count, 2, -1)
    route_share = route_score / jnp.sum(route_score, axis=-1, keepdims=True)
    mixed = jnp.sum(picked.astype(jnp.float32) * route_share[:, :, None], axis=1).astype(
        jnp.bfloat16
    )
    return (gate_ready, up_ready, down_ready, mixed)


def solution(mesh):
    return jax.shard_map(
        on_device,
        mesh=mesh,
        in_specs=(
            P(("gr", "fs"), None),
            P(("gr", "fs")),
            P(None, ("gr", "fs"), "tp"),
            P(None, ("gr", "fs"), "tp"),
            P(None, "tp", ("gr", "fs")),
            P(("gr", "fs"), None),
            P(("gr", "fs"), None),
        ),
        out_specs=(
            P("fs", None, "tp"),
            P("fs", None, "tp"),
            P("fs", "tp", None),
            P(("gr", "fs"), "tp"),
        ),
        check_vma=False,
    )
```

profile of v0, /device:TPU:0, one launch (start us, length us, event | category | flops | bytes accessed | tf_op | source)
XLA Modules:
  0.0 307.5 jit_solution(13147382898146863638)
XLA Ops:
  7.2 3.9 %fusion.16 = (bf16[8,1,128,512]{3,2,1,0:T(8,128)(2,1)}, bf16[8,1,128,512]{3,2,1,0:T(8,128)(2,1)S(1)}) fusion(f32[8,128,512]{2,1,0:T(8,128)} %param.10, f32[128]{0:T(128)} %param.8, f32[8,128,512]{2,1,0:T(8,128)} %param.9), kind=kLoop, calls=%fused_computation.26 | loop fusion | flops 2097152 | bytes 6291968 | tf_op jit(solution)/shard_map/broadcast_in_dim | solution.py:16
  11.0 33.1 %all_to_all.43 = bf16[8,1,128,512]{3,2,1,0:T(8,128)(2,1)} all-to-all(bf16[8,1,128,512]{3,2,1,0:T(8,128)(2,1)S(1)} %get-tuple-element.13), channel_id=1, replica_groups=mesh['gr'=2,'fs'=8,'tp'=2] {'fs'}, dimensions={0} | all-to-all | bytes 2097152 | tf_op jit(solution)/shard_map/all_to_all | solution.py:15
  44.1 3.6 %all-to-all-start.1 = ((bf16[8,1,128,512]{3,2,1,0:T(8,128)(2,1)}), bf16[8,1,128,512]{3,2,1,0:T(8,128)(2,1)S(1)}, u32[]{:S(2)}, u32[]{:S(2)}) async-start(bf16[8,1,128,512]{3,2,1,0:T(8,128)(2,1)} %get-tuple-element.12), calls=%async_computation.1 | async-start | bytes 2097152 | tf_op jit(solution)/shard_map/all_to_all | solution.py:16
  49.9 2.6 copy.47
  52.6 20.7 %all-to-all-done.1 = bf16[8,1,128,512]{3,2,1,0:T(8,128)(2,1)S(1)} async-done(((bf16[8,1,128,512]{3,2,1,0:T(8,128)(2,1)}), bf16[8,1,128,512]{3,2,1,0:T(8,128)(2,1)S(1)}, u32[]{:S(2)}, u32[]{:S(2)}) %all-to-all-start.1) | async-done | bytes 1048608 | tf_op jit(solution)/shard_map/all_to_all | solution.py:16
  73.3 4.3 %all-to-all-start.2 = ((bf16[8,512,1,128]{1,3,2,0:T(8,128)(2,1)}), bf16[8,512,1,128]{1,3,2,0:T(8,128)(2,1)}, u32[]{:S(2)}, u32[]{:S(2)}) async-start(bf16[8,512,1,128]{1,3,2,0:T(8,128)(2,1)} %bitcast.94), calls=%async_computation.2 | async-start | bytes 2097152 | tf_op jit(solution)/shard_map/all_to_all | solution.py:28
  80.6 6.0 %gather_fusion = bf16[1024,2048]{1,0:T(8,128)(2,1)} fusion(bf16[256,2048]{1,0:T(8,128)(2,1)S(1)} %fusion.5, s32[1024]{0:T(1024)S(1)} %fusion.21), kind=kCustom, calls=%fused_computation | custom fusion | bytes 8392704 | tf_op jit(solution)/shard_map/gather | solution.py:56
  89.1 4.5 %broadcast_select_fusion = bf16[8,1,128,2048]{3,2,1,0:T(8,128)(2,1)} fusion(bf16[8,1,128,2048]{3,2,1,0:T(8,128)(2,1)} %bitcast.99, pred[8,128]{1,0:T(8,128)(4,1)S(1)} %bitcast.112), kind=kLoop, calls=%fused_computation.9 | loop fusion | flops 2097152 | bytes 8389632 | tf_op jit(solution)/shard_map/jit(_where)/select_n | solution.py:56
  93.6 9.4 %all-to-all-done.2 = bf16[8,512,1,128]{1,3,2,0:T(8,128)(2,1)} async-done(((bf16[8,512,1,128]{1,3,2,0:T(8,128)(2,1)}), bf16[8,512,1,128]{1,3,2,0:T(8,128)(2,1)}, u32[]{:S(2)}, u32[]{:S(2)}) %all-to-all-start.2) | async-done | bytes 1048608 | tf_op jit(solution)/shard_map/all_to_all | solution.py:28
  103.0 4.5 %all-to-all-start.3 = ((bf16[8,1,128,2048]{3,2,1,0:T(8,128)(2,1)}), bf16[8,1,128,2048]{3,2,1,0:T(8,128)(2,1)}, u32[]{:S(2)}, u32[]{:S(2)}) async-start(bf16[8,1,128,2048]{3,2,1,0:T(8,128)(2,1)} %broadcast_select_fusion), calls=%async_computation.3 | async-start | bytes 8388608 | tf_op jit(solution)/shard_map/all_to_all | solution.py:58
  111.6 33.3 %all-gather.8.cloned.1.call-done = bf16[1,512,2,1024]{3,1,0,2:T(8,128)(2,1)} async-done(((bf16[1,512,1,1024]{3,1,0,2:T(8,128)(2,1)}), bf16[1,512,2,1024]{3,1,0,2:T(8,128)(2,1)}) %all-gather.8.cloned.1.call-update) | async-done | bytes 2097168 | tf_op jit(solution)/shard_map/all_gather | solution.py:30
  144.9 3.7 %copy.56 = bf16[1,512,2,1024]{3,2,1,0:T(2,128)(2,1)S(1)} copy(bf16[1,512,2,1024]{3,1,0,2:T(8,128)(2,1)} %all-gather.8.cloned.1.call-done) | data formatting | bytes 4194304 | tf_op jit(solution)/shard_map/all_gather | solution.py:30
  148.7 2.8 reshape.191
  151.5 28.1 %all-gather.4.cloned.1.call-done = bf16[1,2,1024,512]{3,2,0,1:T(8,128)(2,1)} async-done(((bf16[1,1,1024,512]{3,2,0,1:T(8,128)(2,1)}), bf16[1,2,1024,512]{3,2,0,1:T(8,128)(2,1)}) %all-gather.4.cloned.1.call-update) | async-done | bytes 2097168 | tf_op jit(solution)/shard_map/all_gather | solution.py:21
  179.6 20.3 %all-to-all-done.3 = bf16[8,1,128,2048]{3,2,1,0:T(8,128)(2,1)} async-done(((bf16[8,1,128,2048]{3,2,1,0:T(8,128)(2,1)}), bf16[8,1,128,2048]{3,2,1,0:T(8,128)(2,1)}, u32[]{:S(2)}, u32[]{:S(2)}) %all-to-all-start.3) | async-done | bytes 4194336 | tf_op jit(solution)/shard_map/all_to_all | solution.py:58
  199.8 6.7 %fusion.2 = f32[512,8,128]{2,0,1:T(8,128)} fusion(bf16[2048,512,1]{1,0,2:T(8,128)(2,1)} %bitcast.103, bf16[8,1,128,2048]{3,2,1,0:T(8,128)(2,1)} %all-to-all-done.3), kind=kOutput, calls=%fused_computation.6 | convolution fusion | flops 2147483648 | bytes 8388608 | tf_op jit(solution)/shard_map/seck,ekh->sech/dot_general | solution.py:59
  206.5 8.3 %all-gather.6.cloned.1.call-done = bf16[1,2,1024,512]{3,2,0,1:T(8,128)(2,1)} async-done(((bf16[1,1,1024,512]{3,2,0,1:T(8,128)(2,1)}), bf16[1,2,1024,512]{3,2,0,1:T(8,128)(2,1)}) %all-gather.6.cloned.1.call-update) | async-done | bytes 2097168 | tf_op jit(solution)/shard_map/all_gather | solution.py:21
  214.8 8.9 %convert_bitcast_fusion = bf16[8,1,128,2048]{3,2,0,1:T(8,128)(2,1)} fusion(bf16[512,2048,1]{1,0,2:T(8,128)(2,1)S(1)} %copy-done.4, bf16[2048,512,1]{1,0,2:T(8,128)(2,1)} %bitcast.105, bf16[8,1,128,2048]{3,2,1,0:T(8,128)(2,1)} %all-to-all-done.3, f32[512,8,128]{2,0,1:T(8,128)} %fusion.2), kind=kOutput, calls=%fused_computation.8 | convolution fusion | flops 4300210176 | bytes 14680064 | tf_op jit(solution)/shard_map/sech,ehk->seck/dot_general | solution.py:64
  223.8 12.0 %reduce-scatter.2.cloned.1.call-done = bf16[8,1,128,1024]{3,2,0,1:T(8,128)(2,1)} async-done(((bf16[8,1,128,2048]{3,2,0,1:T(8,128)(2,1)}), bf16[8,1,128,1024]{3,2,0,1:T(8,128)(2,1)}) %reduce-scatter.2.cloned.1.call-update) | async-done | bytes 2097168 | tf_op jit(solution)/shard_map/reduce_scatter | solution.py:67
  235.8 6.0 %all-to-all-start.4 = ((bf16[8,1,128,1024]{3,2,1,0:T(8,128)(2,1)}), bf16[8,1,128,1024]{3,2,1,0:T(8,128)(2,1)S(1)}, u32[]{:S(2)}, u32[]{:S(2)}) async-start(bf16[8,1,128,1024]{3,2,1,0:T(8,128)(2,1)} %bitcast.107), calls=%async_computation.5 | async-start | bytes 4194304 | tf_op jit(solution)/shard_map/all_to_all | solution.py:70
  242.0 3.9 %copy.49 = bf16[1,512,2,1024]{1,3,2,0:T(8,128)(2,1)} copy(bf16[1,512,2,1024]{3,1,0,2:T(8,128)(2,1)} %all-gather.8.cloned.1.call-done) | data formatting | bytes 4194304 | tf_op jit(solution)/shard_map/all_gather | solution.py:30
  246.0 3.9 %copy.60 = bf16[1,512,2048]{2,1,0:T(8,128)(2,1)} copy(bf16[1,512,2048]{1,2,0:T(8,128)(2,1)} %bitcast.100) | data formatting | bytes 4194304
  249.9 40.5 %all-to-all-done.4 = bf16[8,1,128,1024]{3,2,1,0:T(8,128)(2,1)S(1)} async-done(((bf16[8,1,128,1024]{3,2,1,0:T(8,128)(2,1)}), bf16[8,1,128,1024]{3,2,1,0:T(8,128)(2,1)S(1)}, u32[]{:S(2)}, u32[]{:S(2)}) %all-to-all-start.4) | async-done | bytes 2097184 | tf_op jit(solution)/shard_map/all_to_all | solution.py:70
  293.8 3.5 %multiply_reduce_fusion = bf16[256,1024]{1,0:T(8,128)(2,1)} fusion(f32[256,2,1024]{2,1,0:T(2,128)S(1)} %reshape.155, f32[256,2]{1,0:T(8,128)S(1)} %copy.59), kind=kLoop, calls=%fused_computation.21 | loop fusion | flops 786432 | bytes 2623488 | tf_op jit(solution)/shard_map/reduce_sum | solution.py:74
  (52 shorter events, 18.9 us)
Async XLA Ops:
  11.0 36.7 %copy-start.5 = (s32[256,2]{0,1:T(2,128)S(1)}, s32[256,2]{0,1:T(2,128)}, u32[]{:S(2)}) copy-start(s32[256,2]{0,1:T(2,128)} %param.12) | copy-start | bytes 6148
  44.1 29.2 %all-to-all-start.1 = ((bf16[8,1,128,512]{3,2,1,0:T(8,128)(2,1)}), bf16[8,1,128,512]{3,2,1,0:T(8,128)(2,1)S(1)}, u32[]{:S(2)}, u32[]{:S(2)}) async-start(bf16[8,1,128,512]{3,2,1,0:T(8,128)(2,1)} %get-tuple-element.12), calls=%async_computation.1 | async-start | bytes 2097152 | tf_op jit(solution)/shard_map/all_to_all | solution.py:16
  49.9 30.1 %copy-start = (bf16[256,2048]{1,0:T(8,128)(2,1)S(1)}, bf16[256,2048]{1,0:T(8,128)(2,1)}, u32[]{:S(2)}) copy-start(bf16[256,2048]{1,0:T(8,128)(2,1)} %param.7) | copy-start | bytes 3145732
  73.3 7.3 %copy-start.1 = (bf16[8,1,128,512]{3,2,1,0:T(8,128)(2,1)}, bf16[8,1,128,512]{3,2,1,0:T(8,128)(2,1)S(1)}, u32[]{:S(2)}) copy-start(bf16[8,1,128,512]{3,2,1,0:T(8,128)(2,1)S(1)} %all-to-all-done.1) | copy-start | bytes 3145732
  73.3 29.7 %all-to-all-start.2 = ((bf16[8,512,1,128]{1,3,2,0:T(8,128)(2,1)}), bf16[8,512,1,128]{1,3,2,0:T(8,128)(2,1)}, u32[]{:S(2)}, u32[]{:S(2)}) async-start(bf16[8,512,1,128]{1,3,2,0:T(8,128)(2,1)} %bitcast.94), calls=%async_computation.2 | async-start | bytes 2097152 | tf_op jit(solution)/shard_map/all_to_all | solution.py:28
  103.0 96.8 %all-to-all-start.3 = ((bf16[8,1,128,2048]{3,2,1,0:T(8,128)(2,1)}), bf16[8,1,128,2048]{3,2,1,0:T(8,128)(2,1)}, u32[]{:S(2)}, u32[]{:S(2)}) async-start(bf16[8,1,128,2048]{3,2,1,0:T(8,128)(2,1)} %broadcast_select_fusion), calls=%async_computation.3 | async-start | bytes 8388608 | tf_op jit(solution)/shard_map/all_to_all | solution.py:58
  107.6 37.4 %all-gather.8.cloned.1.call-start = ((), (), s32[]{:S(2)}) async-start(), calls=%async_computation.8 | async-start | bytes 3145728 | tf_op jit(solution)/shard_map/all_gather | solution.py:30
  109.9 69.7 %all-gather.4.cloned.1.call-start = ((), (), s32[]{:S(2)}) async-start(), calls=%async_computation.6 | async-start | bytes 3145728 | tf_op jit(solution)/shard_map/all_gather | solution.py:21
  110.7 104.2 %all-gather.6.cloned.1.call-start = ((), (), s32[]{:S(2)}) async-start(), calls=%async_computation.7 | async-start | bytes 3145728 | tf_op jit(solution)/shard_map/all_gather | solution.py:21
  111.4 124.4 %reduce-scatter.2.cloned.1.call-start = ((), (), s32[]{:S(2)}) async-start(), calls=%async_computation.9 | async-start | bytes 6291456 | tf_op jit(solution)/shard_map/reduce_scatter | solution.py:67
  199.8 15.0 %copy-start.4 = (bf16[512,2048,1]{1,0,2:T(8,128)(2,1)S(1)}, bf16[512,2048,1]{1,0,2:T(8,128)(2,1)}, u32[]{:S(2)}) copy-start(bf16[512,2048,1]{1,0,2:T(8,128)(2,1)} %reshape.191) | copy-start | bytes 6291460
  235.8 6.0 %copy-start.6 = (f32[256,2]{0,1:T(2,128)S(1)}, f32[256,2]{0,1:T(2,128)}, u32[]{:S(2)}) copy-start(f32[256,2]{0,1:T(2,128)} %param.13) | copy-start | bytes 6148
  235.8 54.6 %all-to-all-start.4 = ((bf16[8,1,128,1024]{3,2,1,0:T(8,128)(2,1)}), bf16[8,1,128,1024]{3,2,1,0:T(8,128)(2,1)S(1)}, u32[]{:S(2)}, u32[]{:S(2)}) async-start(bf16[8,1,128,1024]{3,2,1,0:T(8,128)(2,1)} %bitcast.107), calls=%async_computation.5 | async-start | bytes 4194304 | tf_op jit(solution)/shard_map/all_to_all | solution.py:70
  293.8 3.5 %copy-start.2 = (bf16[1,2,1024,512]{3,2,0,1:T(8,128)(2,1)S(1)}, bf16[1,2,1024,512]{3,2,0,1:T(8,128)(2,1)}, u32[]{:S(2)}) copy-start(bf16[1,2,1024,512]{3,2,0,1:T(8,128)(2,1)} %all-gather.4.cloned.1.call-done) | copy-start | bytes 6291460
  297.3 2.3 copy-start.3
Sparse Core Ops, SparseCore 0:
  110.5 34.3 all-gather.7
  146.5 33.0 all-gather.3
  181.7 33.0 all-gather.5
  223.9 11.8 reduce-scatter.1
where the time goes:
time: 308 us
  waiting for transfers between devices  174 us (56%)
  local copies, waits for them, and re-layouts  38.3 us (12%)
  blocking collectives  33.1 us (11%)
  starting transfers between devices  18.7 us (6%)
  matrix products  15.6 us (5%)
  between operations  13.9 us (5%)
  other arithmetic  13.7 us (4%)
    all_to_all x1, waiting for transfers between devices, on_device(): lax.all_to_all(summed, 'fs', split_axis=0, concat_axis=0, tiled=True)  40.5 us
    all_gather x2, waiting for transfers between devices, move_inputs(): lax.all_gather(shortened(flattened), 'gr', axis=1, tiled=True)  36.4 us
    all_gather x1, waiting for transfers between devices, move_down(): owned = lax.all_gather(flattened, 'gr', axis=2, tiled=True)  33.3 us
    all_to_all x1, blocking collectives, move_inputs(): lax.all_to_all(gate_cast[:, None], 'fs', split_axis=0, concat_axis=1, til...  33.1 us
    all_to_all x1, waiting for transfers between devices, move_inputs(): lax.all_to_all(up_cast[:, None], 'fs', split_axis=0, concat_axis=1, tiled...  20.7 us
    all_to_all x1, waiting for transfers between devices, on_device(): lax.all_to_all(outgoing, 'fs', split_axis=0, concat_axis=0, tiled=True)  20.3 us
    reduce_scatter x1, waiting for transfers between devices, on_device(): lax.psum_scatter(partial_value.astype(jnp.bfloat16), 'tp', scatter_dimens...  12 us
    unnamed x19, local copies, waits for them, and re-layouts  10.4 us
  transfers between devices with their start and end apart: 8, of which 8 were waited for; matrix products, arithmetic and copies ran while one was open for 14% of the time, Pallas kernels for 0%

commit v1 on v0

v1 whole, which is shorter than its diff:
```python
import jax
import jax.numpy as jnp
from jax import lax
from jax.sharding import PartitionSpec as P

epsilon = 1e-06


def shifted(value, name, step):
    count = lax.axis_size(name)
    return lax.ppermute(value, name, [(i, (i + step) % count) for i in range(count)])


def in_order(own, name):
    count = lax.axis_size(name)
    place = lax.axis_index(name)
    pieces = [own] + [shifted(own, name, step) for step in range(1, count)]
    if count == 1:
        return pieces
    if count == 2:
        return [jnp.where(place == j, pieces[0], pieces[1]) for j in range(2)]
    return [lax.select_n((place - j) % count, *pieces) for j in range(count)]


def on_device(tokens, norm_gain, gate_train, up_train, down_train, expert_ids, route_score):
    fs_count = lax.axis_size("fs")
    tp_count = lax.axis_size("tp")
    tp_place = lax.axis_index("tp")
    experts, rows, hidden_width = gate_train.shape
    tok_count, width = tokens.shape
    capacity = 4 * tok_count // experts
    served = experts // fs_count
    half = fs_count // 2
    half_experts = half * served
    part = width // tp_count

    gate_cast = (norm_gain[None, :, None] * gate_train).astype(jnp.bfloat16)
    up_cast = (norm_gain[None, :, None] * up_train).astype(jnp.bfloat16)
    down_cast = down_train.astype(jnp.bfloat16)
    both_cast = jnp.stack([gate_cast, up_cast], axis=1)
    both = lax.all_to_all(both_cast, "fs", split_axis=0, concat_axis=0, tiled=True)
    both = both.reshape(fs_count, served, 2, rows, hidden_width)

    floated = tokens.astype(jnp.float32)
    scale = lax.rsqrt(jnp.mean(floated * floated, axis=-1, keepdims=True) + epsilon)
    share = lax.dynamic_slice_in_dim(tokens, tp_place * part, part, axis=1)
    normed = (share.astype(jnp.float32) * scale).astype(jnp.bfloat16)
    flat_ids = expert_ids.reshape(-1)
    matches = (flat_ids[:, None] == jnp.arange(experts, dtype=jnp.int32)[None, :]).astype(jnp.int32)
    ranked = jnp.sum((jnp.cumsum(matches, axis=0) - 1) * matches, axis=1)
    slot_index = flat_ids * capacity + ranked
    pick_token = jnp.arange(flat_ids.shape[0], dtype=jnp.int32) // 2
    slot_token = jnp.zeros((experts * capacity,), jnp.int32).at[slot_index].set(pick_token)
    mirror_rows = shifted(normed, "fs", half)
    mirror_slots = shifted(slot_token, "fs", half)
    upper = lax.axis_index("fs") // half
    own_slots = lax.dynamic_slice_in_dim(
        slot_token.reshape(2, half_experts, capacity), upper, 1, axis=0
    )[0]
    far_slots = lax.dynamic_slice_in_dim(
        mirror_slots.reshape(2, half_experts, capacity), upper, 1, axis=0
    )[0] + tok_count
    first = jnp.where(upper == 0, own_slots, far_slots)
    second = jnp.where(upper == 0, far_slots, own_slots)
    pool = jnp.concatenate([normed, mirror_rows], axis=0)
    chosen = jnp.stack([first, second], axis=1).reshape(-1)
    outgoing = pool[chosen].reshape(half_experts, 2, capacity, part)

    down_cast, both = lax.optimization_barrier((down_cast, both))
    down = lax.all_to_all(down_cast, "fs", split_axis=0, concat_axis=0, tiled=True)
    down = down.reshape(fs_count, served, hidden_width, rows)
    outgoing, down = lax.optimization_barrier((outgoing, down))
    groups = [list(range(half)), list(range(half, 2 * half))]
    received = lax.all_to_all(
        outgoing, "fs", split_axis=0, concat_axis=0, tiled=True, axis_index_groups=groups
    )
    received = received.reshape(half, served, 2, capacity, part)
    by_expert = received.transpose(1, 0, 2, 3, 4).reshape(served, half * 2 * capacity, part)

    both_parts = in_order(both, "gr")
    gate_ready = jnp.concatenate(
        [p[:, :, 0].transpose(1, 0, 2, 3).reshape(served, -1, hidden_width) for p in both_parts], axis=1
    )
    up_ready = jnp.concatenate(
        [p[:, :, 1].transpose(1, 0, 2, 3).reshape(served, -1, hidden_width) for p in both_parts], axis=1
    )
    down_parts = in_order(down, "gr")
    down_ready = jnp.concatenate(
        [p.transpose(1, 2, 0, 3).reshape(served, hidden_width, -1) for p in down_parts], axis=2
    )

    gate_act = up_act = 0.0
    for step in range(tp_count):
        piece = shifted(by_expert, "tp", step) if step else by_expert
        start = ((tp_place - step) % tp_count) * part
        gate_piece = lax.dynamic_slice_in_dim(gate_ready, start, part, axis=1)
        up_piece = lax.dynamic_slice_in_dim(up_ready, start, part, axis=1)
        gate_act = gate_act + jnp.einsum(
            "enk,ekh->enh", piece, gate_piece, preferred_element_type=jnp.float32
        )
        up_act = up_act + jnp.einsum(
            "enk,ekh->enh", piece, up_piece, preferred_element_type=jnp.float32
        )
    hidden = (jax.nn.silu(gate_act) * up_act).astype(jnp.bfloat16)
    summed = 0.0
    for step in range(tp_count):
        start = ((tp_place + step) % tp_count) * part
        down_piece = lax.dynamic_slice_in_dim(down_ready, start, part, axis=2)
        value = jnp.einsum(
            "enh,ehk->enk", hidden, down_piece, preferred_element_type=jnp.float32
        ).astype(jnp.bfloat16)
        value = shifted(value, "tp", step) if step else value
        summed = summed + value.astype(jnp.float32)
    expert_out = summed.astype(jnp.bfloat16).reshape(served, half, 2, capacity, part)
    leaving = expert_out.transpose(2, 1, 0, 3, 4).reshape(experts, capacity, part)
    returned = lax.all_to_all(leaving, "fs", split_axis=0, concat_axis=0, tiled=True)
    flat_back = returned.reshape(experts * capacity, part)
    picked = flat_back[slot_index].reshape(tok_count, 2, part)
    route_share = route_score / jnp.sum(route_score, axis=-1, keepdims=True)
    mixed = jnp.sum(picked.astype(jnp.float32) * route_share[:, :, None], axis=1).astype(
        jnp.bfloat16
    )
    return (gate_ready, up_ready, down_ready, mixed)


def solution(mesh):
    return jax.shard_map(
        on_device,
        mesh=mesh,
        in_specs=(
            P(("gr", "fs"), None),
            P(("gr", "fs")),
            P(None, ("gr", "fs"), "tp"),
            P(None, ("gr", "fs"), "tp"),
            P(None, "tp", ("gr", "fs")),
            P(("gr", "fs"), None),
            P(("gr", "fs"), None),
        ),
        out_specs=(
            P("fs", None, "tp"),
            P("fs", None, "tp"),
            P("fs", "tp", None),
            P(("gr", "fs"), "tp"),
        ),
        check_vma=False,
    )
```

time: 308 us -> 275 us (0.89)
  blocking collectives: 33.1 us -> 0 us
  local copies, waits for them, and re-layouts: 38.3 us -> 14.3 us
  waiting for transfers between devices: 174 us -> 197 us
  between operations: 13.9 us -> 0.93 us
  other arithmetic: 13.7 us -> 22.6 us
  starting transfers between devices: 18.7 us -> 26.5 us
    ppermute x0 -> x6, waiting for transfers between devices: none -> 87.7 us  [shifted(): lax.ppermute(value, name, [(i, (i + step) % count) for i in range(count)])]
    all_gather x3 -> x0, waiting for transfers between devices: 69.7 us -> none  [the longest x2 36.4 us: move_inputs(): lax.all_gather(shortened(flattened), 'gr', axis=1, tiled=True)]
    all_to_all x1 -> x0, blocking collectives: 33.1 us -> none  [move_inputs(): lax.all_to_all(gate_cast[:, None], 'fs', split_axis=0, concat_axis=1, til...]
    all_to_all x4, waiting for transfers between devices: 90.9 us -> 110 us  [the longest x1 43.8 us: on_device(): lax.all_to_all(both_cast, 'fs', split_axis=0, concat_axis=0, tiled=True)]
    reduce_scatter x1 -> x0, waiting for transfers between devices: 12 us -> none  [on_device(): lax.psum_scatter(partial_value.astype(jnp.bfloat16), 'tp', scatter_dimens...]
    unnamed x19 -> x18, local copies, waits for them, and re-layouts: 10.4 us -> 0.32 us
    all_gather x2 -> x0, local copies, waits for them, and re-layouts: 7.69 us -> none  [move_down(): owned = lax.all_gather(flattened, 'gr', axis=2, tiled=True)]
    concatenate x0 -> x3, other arithmetic: none -> 5.81 us  [the longest x1 3.08 us: on_device(): jnp.concatenate([p[:, :, 1].transpose(1, 0, 2, 3).reshape(served, -1, hid...]
  transfers between devices with their start and end apart: 8 -> 10, of which waited for: 8 -> 8; matrix products, arithmetic and copies ran while one was open for 14% -> 11% of each run, Pallas kernels for 0% -> 0%
where the time goes in v1:
time: 275 us; the launch traced here: 274 us
  waiting for transfers between devices  197 us (72%)
  starting transfers between devices  26.5 us (10%)
  other arithmetic  22.6 us (8%)
  local copies, waits for them, and re-layouts  14.3 us (5%)
  matrix products  12.6 us (5%)
    ppermute x6, waiting for transfers between devices, shifted(): lax.ppermute(value, name, [(i, (i + step) % count) for i in range(count)])  87.7 us
    all_to_all x1, waiting for transfers between devices, on_device(): lax.all_to_all(both_cast, 'fs', split_axis=0, concat_axis=0, tiled=True)  43.8 us
    all_to_all x1, waiting for transfers between devices, on_device(): lax.all_to_all(leaving, 'fs', split_axis=0, concat_axis=0, tiled=True)  43.8 us
    all_to_all x1, waiting for transfers between devices, on_device(): lax.all_to_all(outgoing, 'fs', split_axis=0, concat_axis=0, tiled=True, a...  21.9 us
    all_to_all x1, starting transfers between devices, on_device(): lax.all_to_all(both_cast, 'fs', split_axis=0, concat_axis=0, tiled=True)  7.44 us
  transfers between devices with their start and end apart: 10, of which 8 were waited for; matrix products, arithmetic and copies ran while one was open for 11% of the time, Pallas kernels for 0%

profile of v1, /device:TPU:0, one launch (start us, length us, event | category | flops | bytes accessed | tf_op | source)
XLA Modules:
  0.0 274.1 jit_solution(3214755654261403710)
XLA Ops:
  0.6 2.9 %fusion.7 = (bf16[8,1,128,512]{3,2,1,0:T(8,128)(2,1)S(1)}, bf16[8,1,128,512]{3,2,1,0:T(8,128)(2,1)S(1)}) fusion(f32[8,128,512]{2,1,0:T(8,128)} %param.9, f32[128]{0:T(128)} %param.8, f32[8,128,512]{2,1,0:T(8,128)} %param.10), kind=kLoop, calls=%fused_computation.28 | loop fusion | flops 2097152 | bytes 6291968 | tf_op jit(solution)/shard_map/stack | solution.py:40
  5.0 7.4 %all-to-all-start = ((bf16[8,2,128,512]{3,2,1,0:T(8,128)(2,1)}), bf16[8,2,128,512]{3,2,1,0:T(8,128)(2,1)S(1)}, u32[]{:S(2)}, u32[]{:S(2)}) async-start(bf16[8,2,128,512]{3,2,1,0:T(8,128)(2,1)} %pad_maximum_fusion.2), calls=%async_computation | async-start | bytes 4194304 | tf_op jit(solution)/shard_map/all_to_all | solution.py:41
  12.8 2.7 convert_element_type.58
  16.9 43.8 %all-to-all-done = bf16[8,2,128,512]{3,2,1,0:T(8,128)(2,1)S(1)} async-done(((bf16[8,2,128,512]{3,2,1,0:T(8,128)(2,1)}), bf16[8,2,128,512]{3,2,1,0:T(8,128)(2,1)S(1)}, u32[]{:S(2)}, u32[]{:S(2)}) %all-to-all-start) | async-done | bytes 2097184 | tf_op jit(solution)/shard_map/all_to_all | solution.py:41
  60.7 4.2 %all-to-all-start.1 = ((bf16[8,512,128]{2,1,0:T(8,128)(2,1)}), bf16[8,512,128]{2,1,0:T(8,128)(2,1)}, u32[]{:S(2)}, u32[]{:S(2)}) async-start(bf16[8,512,128]{2,1,0:T(8,128)(2,1)} %convert_element_type.58), calls=%async_computation.1 | async-start | bytes 2097152 | tf_op jit(solution)/shard_map/all_to_all | solution.py:70
  65.5 2.4 scatter_custom_fusion
  68.0 2.9 %collective-permute-start.2 = (s32[1024]{0:T(1024)S(1)}, s32[1024]{0:T(1024)S(1)}, u32[]{:S(2)}, u32[]{:S(2)}) collective-permute-start(s32[1024]{0:T(1024)S(1)} %scatter_custom_fusion), channel_id=1, source_target_pairs={{0,8},{2,10},{4,12},{6,14},{8,0},{10,2},{12,4},{14,6},{1,9},{3,11}... | collective-permute-start | bytes 12296 | tf_op jit(solution)/shard_map/ppermute | solution.py:11
  72.2 31.2 %collective-permute-done.2 = s32[1024]{0:T(1024)S(1)} collective-permute-done((s32[1024]{0:T(1024)S(1)}, s32[1024]{0:T(1024)S(1)}, u32[]{:S(2)}, u32[]{:S(2)}) %collective-permute-start.2) | collective-permute-done | bytes 4128 | tf_op jit(solution)/shard_map/ppermute | solution.py:11
  103.5 9.7 %collective-permute-done.1 = bf16[256,1024]{1,0:T(8,128)(2,1)} collective-permute-done((bf16[256,1024]{1,0:T(8,128)(2,1)}, bf16[256,1024]{1,0:T(8,128)(2,1)}, u32[]{:S(2)}, u32[]{:S(2)}) %collective-permute-start.1) | collective-permute-done | bytes 524320 | tf_op jit(solution)/shard_map/ppermute | solution.py:11
  114.5 5.3 %gather_fusion = bf16[1024,1024]{1,0:T(8,128)(2,1)} fusion(bf16[512,1024]{1,0:T(8,128)(2,1)S(1)} %pad_maximum_fusion.3, s32[1024]{0:T(1024)S(1)} %broadcast_clamp_fusion), kind=kCustom, calls=%fused_computation | custom fusion | bytes 4198400 | tf_op jit(solution)/shard_map/gather | solution.py:67
  119.8 4.6 %all-to-all-start.2 = ((bf16[4,2,128,1024]{3,2,1,0:T(8,128)(2,1)}), bf16[4,2,128,1024]{3,2,1,0:T(8,128)(2,1)}, u32[]{:S(2)}, u32[]{:S(2)}) async-start(bf16[4,2,128,1024]{3,2,1,0:T(8,128)(2,1)} %bitcast.83), calls=%async_computation.2 | async-start | bytes 4194304 | tf_op jit(solution)/shard_map/all_to_all | solution.py:74
  126.6 21.9 %all-to-all-done.2 = bf16[4,2,128,1024]{3,2,1,0:T(8,128)(2,1)} async-done(((bf16[4,2,128,1024]{3,2,1,0:T(8,128)(2,1)}), bf16[4,2,128,1024]{3,2,1,0:T(8,128)(2,1)}, u32[]{:S(2)}, u32[]{:S(2)}) %all-to-all-start.2) | async-done | bytes 2097184 | tf_op jit(solution)/shard_map/all_to_all | solution.py:74
  148.5 24.7 %collective-permute-done = bf16[8,1,2,128,512]{4,3,2,0,1:T(8,128)(2,1)} collective-permute-done((bf16[8,1,2,128,512]{4,3,2,0,1:T(8,128)(2,1)S(1)}, bf16[8,1,2,128,512]{4,3,2,0,1:T(8,128)(2,1)}, u32[]{:S(2)}, u32[]{:S(2)}) %collective-permute-start) | collective-permute-done | bytes 2097184 | tf_op jit(solution)/shard_map/ppermute | solution.py:11
  173.1 1.9 broadcast_select_fusion.1
  175.3 17.9 %collective-permute-done.3 = bf16[8,1,512,128]{3,2,0,1:T(8,128)(2,1)} collective-permute-done((bf16[8,1,512,128]{3,2,0,1:T(8,128)(2,1)}, bf16[8,1,512,128]{3,2,0,1:T(8,128)(2,1)}, u32[]{:S(2)}, u32[]{:S(2)}) %collective-permute-start.3) | collective-permute-done | bytes 1048608 | tf_op jit(solution)/shard_map/ppermute | solution.py:11
  195.2 3.8 %fusion.18 = f32[1024,512]{1,0:T(8,128)S(1)} fusion(bf16[1024,1024]{1,0:T(8,128)(2,1)} %bitcast.23, s32[]{:T(128)S(6)} %select_n.146, bf16[1,1024,512]{2,1,0:T(8,128)(2,1)S(1)} %bitcast.85, bf16[1,1024,512]{2,1,0:T(8,128)(2,1)S(1)} %bitcast.88), kind=kOutput, calls=%fused_computation.37 | convolution fusion | flops 1075838976 | bytes 6291460 | tf_op jit(solution)/shard_map/enk,ekh->enh/dot_general | solution.py:98
  199.0 3.0 %fusion.11 = f32[1024,512]{1,0:T(8,128)S(1)} fusion(bf16[1024,1024]{1,0:T(8,128)(2,1)} %bitcast.23, s32[]{:T(128)S(6)} %select_n.146, bf16[1,1024,512]{2,1,0:T(8,128)(2,1)S(1)} %bitcast.91, bf16[1,1024,512]{2,1,0:T(8,128)(2,1)S(1)} %bitcast.94), kind=kOutput, calls=%fused_computation.32 | convolution fusion | flops 1075838976 | bytes 6291460 | tf_op jit(solution)/shard_map/enk,ekh->enh/dot_general | solution.py:101
  203.6 1.8 multiply_convert_fusion
  206.7 4.1 %collective-permute-done.5 = bf16[1,1024,1024]{2,1,0:T(8,128)(2,1)S(1)} collective-permute-done((bf16[1,1024,1024]{2,1,0:T(8,128)(2,1)S(1)}, bf16[1,1024,1024]{2,1,0:T(8,128)(2,1)S(1)}, u32[]{:S(2)}, u32[]{:S(2)}) %collective-permute-start.5) | collective-permute-done | bytes 2097184 | tf_op jit(solution)/shard_map/ppermute | solution.py:11
  213.7 5.0 %all-to-all-start.3 = ((bf16[8,128,1024]{2,1,0:T(8,128)(2,1)}), bf16[8,128,1024]{2,1,0:T(8,128)(2,1)S(1)}, u32[]{:S(2)}, u32[]{:S(2)}) async-start(bf16[8,128,1024]{2,1,0:T(8,128)(2,1)} %bitcast.84), calls=%async_computation.3 | async-start | bytes 4194304 | tf_op jit(solution)/shard_map/all_to_all | solution.py:116
  218.9 3.1 %pad_maximum_fusion.1 = bf16[1,2048,512]{2,1,0:T(8,128)(2,1)} fusion(bf16[1,1024,512]{2,1,0:T(8,128)(2,1)} %bitcast.96, bf16[1,1024,512]{2,1,0:T(8,128)(2,1)} %bitcast.93), kind=kLoop, calls=%fused_computation.12 | loop fusion | flops 4194304 | bytes 4194304 | tf_op jit(solution)/shard_map/concatenate | solution.py:84
  223.4 43.8 %all-to-all-done.3 = bf16[8,128,1024]{2,1,0:T(8,128)(2,1)S(1)} async-done(((bf16[8,128,1024]{2,1,0:T(8,128)(2,1)}), bf16[8,128,1024]{2,1,0:T(8,128)(2,1)S(1)}, u32[]{:S(2)}, u32[]{:S(2)}) %all-to-all-start.3) | async-done | bytes 2097184 | tf_op jit(solution)/shard_map/all_to_all | solution.py:116
  267.2 2.0 gather_fusion.1
  270.6 3.5 %multiply_reduce_fusion = bf16[256,1024]{1,0:T(8,128)(2,1)} fusion(f32[256,2,1024]{2,1,0:T(2,128)S(1)} %reshape.243, f32[256,2]{1,0:T(8,128)S(1)} %copy.30), kind=kLoop, calls=%fused_computation.20 | loop fusion | flops 786432 | bytes 2623488 | tf_op jit(solution)/shard_map/reduce_sum | solution.py:120
  (60 shorter events, 19.3 us)
Async XLA Ops:
  5.0 7.4 %copy-start.6 = (s32[256,2]{0,1:T(2,128)S(1)}, s32[256,2]{0,1:T(2,128)}, u32[]{:S(2)}) copy-start(s32[256,2]{0,1:T(2,128)} %param.12) | copy-start | bytes 6148
  5.0 55.7 %all-to-all-start = ((bf16[8,2,128,512]{3,2,1,0:T(8,128)(2,1)}), bf16[8,2,128,512]{3,2,1,0:T(8,128)(2,1)S(1)}, u32[]{:S(2)}, u32[]{:S(2)}) async-start(bf16[8,2,128,512]{3,2,1,0:T(8,128)(2,1)} %pad_maximum_fusion.2), calls=%async_computation | async-start | bytes 4194304 | tf_op jit(solution)/shard_map/all_to_all | solution.py:41
  15.5 55.4 %copy-start.4 = (bf16[256,2048]{1,0:T(8,128)(2,1)S(1)}, bf16[256,2048]{1,0:T(8,128)(2,1)}, u32[]{:S(2)}) copy-start(bf16[256,2048]{1,0:T(8,128)(2,1)} %param.7) | copy-start | bytes 3145732
  60.7 59.1 %all-to-all-start.1 = ((bf16[8,512,128]{2,1,0:T(8,128)(2,1)}), bf16[8,512,128]{2,1,0:T(8,128)(2,1)}, u32[]{:S(2)}, u32[]{:S(2)}) async-start(bf16[8,512,128]{2,1,0:T(8,128)(2,1)} %convert_element_type.58), calls=%async_computation.1 | async-start | bytes 2097152 | tf_op jit(solution)/shard_map/all_to_all | solution.py:70
  68.0 35.4 %collective-permute-start.2 = (s32[1024]{0:T(1024)S(1)}, s32[1024]{0:T(1024)S(1)}, u32[]{:S(2)}, u32[]{:S(2)}) collective-permute-start(s32[1024]{0:T(1024)S(1)} %scatter_custom_fusion), channel_id=1, source_target_pairs={{0,8},{2,10},{4,12},{6,14},{8,0},{10,2},{12,4},{14,6},{1,9},{3,11}... | collective-permute-start | bytes 12296 | tf_op jit(solution)/shard_map/ppermute | solution.py:11
  72.1 41.1 %collective-permute-start.1 = (bf16[256,1024]{1,0:T(8,128)(2,1)}, bf16[256,1024]{1,0:T(8,128)(2,1)}, u32[]{:S(2)}, u32[]{:S(2)}) collective-permute-start(bf16[256,1024]{1,0:T(8,128)(2,1)} %multiply_convert_fusion.3), channel_id=1, source_target_pairs={{0,8},{2,10},{4,12},{6,14},{8,0},{10,2},{12,4},{14,6},{1,9},{3,11}... | collective-permute-start | bytes 1572872 | tf_op jit(solution)/shard_map/ppermute | solution.py:11
  119.8 28.6 %all-to-all-start.2 = ((bf16[4,2,128,1024]{3,2,1,0:T(8,128)(2,1)}), bf16[4,2,128,1024]{3,2,1,0:T(8,128)(2,1)}, u32[]{:S(2)}, u32[]{:S(2)}) async-start(bf16[4,2,128,1024]{3,2,1,0:T(8,128)(2,1)} %bitcast.83), calls=%async_computation.2 | async-start | bytes 4194304 | tf_op jit(solution)/shard_map/all_to_all | solution.py:74
  124.5 48.7 %collective-permute-start = (bf16[8,1,2,128,512]{4,3,2,0,1:T(8,128)(2,1)S(1)}, bf16[8,1,2,128,512]{4,3,2,0,1:T(8,128)(2,1)}, u32[]{:S(2)}, u32[]{:S(2)}) collective-permute-start(bf16[8,1,2,128,512]{4,3,2,0,1:T(8,128)(2,1)S(1)} %bitcast.81), channel_id=1, source_target_pairs={{0,16},{16,0},{1,17},{17,1},{2,18},{18,2},{3,19},{19,3},{4,20},{20... | collective-permute-start | bytes 6291464 | tf_op jit(solution)/shard_map/ppermute | solution.py:11
  126.0 67.2 %collective-permute-start.3 = (bf16[8,1,512,128]{3,2,0,1:T(8,128)(2,1)}, bf16[8,1,512,128]{3,2,0,1:T(8,128)(2,1)}, u32[]{:S(2)}, u32[]{:S(2)}) collective-permute-start(bf16[8,1,512,128]{3,2,0,1:T(8,128)(2,1)} %bitcast.20), channel_id=1, source_target_pairs={{0,16},{16,0},{1,17},{17,1},{2,18},{18,2},{3,19},{19,3},{4,20},{20... | collective-permute-start | bytes 3145736 | tf_op jit(solution)/shard_map/ppermute | solution.py:11
  148.4 53.6 %collective-permute-start.4 = (bf16[1,1024,1024]{2,1,0:T(8,128)(2,1)}, bf16[1,1024,1024]{2,1,0:T(8,128)(2,1)S(1)}, u32[]{:S(2)}, u32[]{:S(2)}) collective-permute-start(bf16[1,1024,1024]{2,1,0:T(8,128)(2,1)} %bitcast.25), channel_id=1, source_target_pairs={{0,1},{1,0},{2,3},{3,2},{4,5},{5,4},{6,7},{7,6},{8,9},{9,8},{10,11... | collective-permute-start | bytes 6291464 | tf_op jit(solution)/shard_map/ppermute | solution.py:11
  175.3 26.8 %copy-start = (bf16[8,1,1,128,512]{4,3,2,0,1:T(8,128)(2,1)}, bf16[8,1,1,128,512]{4,3,2,0,1:T(8,128)(2,1)S(1)}, u32[]{:S(2)}) copy-start(bf16[8,1,1,128,512]{4,3,2,0,1:T(8,128)(2,1)S(1)} %get-tuple-element.24) | copy-start | bytes 3145732
  175.3 28.3 %copy-start.2 = (bf16[8,1,1,128,512]{4,3,2,0,1:T(8,128)(2,1)}, bf16[8,1,1,128,512]{4,3,2,0,1:T(8,128)(2,1)S(1)}, u32[]{:S(2)}) copy-start(bf16[8,1,1,128,512]{4,3,2,0,1:T(8,128)(2,1)S(1)} %get-tuple-element.16) | copy-start | bytes 3145732
  175.3 28.3 %copy-start.3 = (bf16[8,1,1,128,512]{4,3,2,0,1:T(8,128)(2,1)}, bf16[8,1,1,128,512]{4,3,2,0,1:T(8,128)(2,1)S(1)}, u32[]{:S(2)}) copy-start(bf16[8,1,1,128,512]{4,3,2,0,1:T(8,128)(2,1)S(1)} %get-tuple-element.25) | copy-start | bytes 3145732
  195.2 15.7 %copy-start.5 = (bf16[1,512,2048]{2,1,0:T(8,128)(2,1)}, bf16[1,512,2048]{2,1,0:T(8,128)(2,1)S(1)}, u32[]{:S(2)}) copy-start(bf16[1,512,2048]{2,1,0:T(8,128)(2,1)S(1)} %bitcast_dynamic-update-slice_fusion) | copy-start | bytes 6291460
  206.7 4.2 %collective-permute-start.5 = (bf16[1,1024,1024]{2,1,0:T(8,128)(2,1)S(1)}, bf16[1,1024,1024]{2,1,0:T(8,128)(2,1)S(1)}, u32[]{:S(2)}, u32[]{:S(2)}) collective-permute-start(bf16[1,1024,1024]{2,1,0:T(8,128)(2,1)S(1)} %convert_bitcast_fusion), channel_id=1, source_target_pairs={{0,1},{1,0},{2,3},{3,2},{4,5},{5,4},{6,7},{7,6},{8,9},{9,8},{10,11... | collective-permute-start | bytes 6291464 | tf_op jit(solution)/shard_map/ppermute | solution.py:11
  213.7 5.0 %copy-start.7 = (f32[256,2]{0,1:T(2,128)S(1)}, f32[256,2]{0,1:T(2,128)}, u32[]{:S(2)}) copy-start(f32[256,2]{0,1:T(2,128)} %param.13) | copy-start | bytes 6148
  213.7 53.5 %all-to-all-start.3 = ((bf16[8,128,1024]{2,1,0:T(8,128)(2,1)}), bf16[8,128,1024]{2,1,0:T(8,128)(2,1)S(1)}, u32[]{:S(2)}, u32[]{:S(2)}) async-start(bf16[8,128,1024]{2,1,0:T(8,128)(2,1)} %bitcast.84), calls=%async_computation.3 | async-start | bytes 4194304 | tf_op jit(solution)/shard_map/all_to_all | solution.py:116
  218.9 3.1 %copy-start.1 = (bf16[8,1,1,128,512]{4,3,2,0,1:T(8,128)(2,1)S(1)}, bf16[8,1,1,128,512]{4,3,2,0,1:T(8,128)(2,1)}, u32[]{:S(2)}) copy-start(bf16[8,1,1,128,512]{4,3,2,0,1:T(8,128)(2,1)} %copy-done) | copy-start | bytes 3145732

commit v2 on v1

--- a/solution.py
+++ b/solution.py
@@ -54,28 +54,30 @@
     mirror_rows = shifted(normed, "fs", half)
     mirror_slots = shifted(slot_token, "fs", half)
     upper = lax.axis_index("fs") // half
-    own_slots = lax.dynamic_slice_in_dim(
-        slot_token.reshape(2, half_experts, capacity), upper, 1, axis=0
-    )[0]
-    far_slots = lax.dynamic_slice_in_dim(
-        mirror_slots.reshape(2, half_experts, capacity), upper, 1, axis=0
-    )[0] + tok_count
-    first = jnp.where(upper == 0, own_slots, far_slots)
-    second = jnp.where(upper == 0, far_slots, own_slots)
-    pool = jnp.concatenate([normed, mirror_rows], axis=0)
-    chosen = jnp.stack([first, second], axis=1).reshape(-1)
-    outgoing = pool[chosen].reshape(half_experts, 2, capacity, part)
 
-    down_cast, both = lax.optimization_barrier((down_cast, both))
+    def rows_for_half(pool, slots):
+        mine = lax.dynamic_slice_in_dim(
+            slots.reshape(2, half_experts * capacity), upper, 1, axis=0
+        )[0]
+        return pool[mine].reshape(half_experts, capacity, part)
+
+    def over_half(outgoing):
+        groups = [list(range(half)), list(range(half, 2 * half))]
+        received = lax.all_to_all(
+            outgoing, "fs", split_axis=0, concat_axis=0, tiled=True, axis_index_groups=groups
+        )
+        received = received.reshape(half, served, capacity, part)
+        return received.transpose(1, 0, 2, 3).reshape(served, half * capacity, part)
+
+    near_rows = rows_for_half(normed, slot_token)
+    near_rows, both = lax.optimization_barrier((near_rows, both))
+    near = over_half(near_rows)
+    down_cast, near = lax.optimization_barrier((down_cast, near))
     down = lax.all_to_all(down_cast, "fs", split_axis=0, concat_axis=0, tiled=True)
     down = down.reshape(fs_count, served, hidden_width, rows)
-    outgoing, down = lax.optimization_barrier((outgoing, down))
-    groups = [list(range(half)), list(range(half, 2 * half))]
-    received = lax.all_to_all(
-        outgoing, "fs", split_axis=0, concat_axis=0, tiled=True, axis_index_groups=groups
-    )
-    received = received.reshape(half, served, 2, capacity, part)
-    by_expert = received.transpose(1, 0, 2, 3, 4).reshape(served, half * 2 * capacity, part)
+    far_rows = rows_for_half(mirror_rows, mirror_slots)
+    far_rows, down = lax.optimization_barrier((far_rows, down))
+    far = over_half(far_rows)
 
     both_parts = in_order(both, "gr")
     gate_ready = jnp.concatenate(
@@ -89,19 +91,30 @@
         [p.transpose(1, 2, 0, 3).reshape(served, hidden_width, -1) for p in down_parts], axis=2
     )
 
-    gate_act = up_act = 0.0
-    for step in range(tp_count):
-        piece = shifted(by_expert, "tp", step) if step else by_expert
-        start = ((tp_place - step) % tp_count) * part
-        gate_piece = lax.dynamic_slice_in_dim(gate_ready, start, part, axis=1)
-        up_piece = lax.dynamic_slice_in_dim(up_ready, start, part, axis=1)
-        gate_act = gate_act + jnp.einsum(
-            "enk,ekh->enh", piece, gate_piece, preferred_element_type=jnp.float32
-        )
-        up_act = up_act + jnp.einsum(
-            "enk,ekh->enh", piece, up_piece, preferred_element_type=jnp.float32
-        )
-    hidden = (jax.nn.silu(gate_act) * up_act).astype(jnp.bfloat16)
+    def hidden_of(by_expert):
+        gate_act = up_act = 0.0
+        for step in range(tp_count):
+            piece = shifted(by_expert, "tp", step) if step else by_expert
+            start = ((tp_place - step) % tp_count) * part
+            gate_piece = lax.dynamic_slice_in_dim(gate_ready, start, part, axis=1)
+            up_piece = lax.dynamic_slice_in_dim(up_ready, start, part, axis=1)
+            gate_act = gate_act + jnp.einsum(
+                "enk,ekh->enh", piece, gate_piece, preferred_element_type=jnp.float32
+            )
+            up_act = up_act + jnp.einsum(
+                "enk,ekh->enh", piece, up_piece, preferred_element_type=jnp.float32
+            )
+        return (jax.nn.silu(gate_act) * up_act).astype(jnp.bfloat16)
+
+    near_hidden = hidden_of(near)
+    far_hidden = hidden_of(far)
+    hidden = jnp.concatenate(
+        [
+            jnp.where(upper == 0, near_hidden, far_hidden),
+            jnp.where(upper == 0, far_hidden, near_hidden),
+        ],
+        axis=1,
+    )
     summed = 0.0
     for step in range(tp_count):
         start = ((tp_place + step) % tp_count) * part
@@ -111,8 +124,8 @@
         ).astype(jnp.bfloat16)
         value = shifted(value, "tp", step) if step else value
         summed = summed + value.astype(jnp.float32)
-    expert_out = summed.astype(jnp.bfloat16).reshape(served, half, 2, capacity, part)
-    leaving = expert_out.transpose(2, 1, 0, 3, 4).reshape(experts, capacity, part)
+    expert_out = summed.astype(jnp.bfloat16).reshape(served, fs_count, capacity, part)
+    leaving = expert_out.transpose(1, 0, 2, 3).reshape(experts, capacity, part)
     returned = lax.all_to_all(leaving, "fs", split_axis=0, concat_axis=0, tiled=True)
     flat_back = returned.reshape(experts * capacity, part)
     picked = flat_back[slot_index].reshape(tok_count, 2, part)

time: 275 us -> 250 us (0.909)
  waiting for transfers between devices: 197 us -> 155 us
  matrix products: 12.6 us -> 25.5 us
  starting transfers between devices: 26.5 us -> 30.9 us
    ppermute x6 -> x7, waiting for transfers between devices: 87.7 us -> 62.6 us  [shifted(): lax.ppermute(value, name, [(i, (i + step) % count) for i in range(count)])]
    all_to_all x1 -> x2, waiting for transfers between devices: 21.9 us -> 8.67 us  [over_half(): lax.all_to_all(outgoing, 'fs', split_axis=0, concat_axis=0, tiled=True, a...]
    dot_general x4 -> x8, matrix products: 10.1 us -> 21.4 us  [the longest x4 11.3 us: hidden_of(): jnp.einsum('enk,ekh->enh', piece, gate_piece, preferred_element_type=jnp....]
    all_to_all x1, waiting for transfers between devices: 43.8 us -> 39.2 us  [on_device(): lax.all_to_all(both_cast, 'fs', split_axis=0, concat_axis=0, tiled=True)]
    all_to_all x1 -> x2, starting transfers between devices: 4.63 us -> 8.7 us  [over_half(): lax.all_to_all(outgoing, 'fs', split_axis=0, concat_axis=0, tiled=True, a...]
    ppermute x6 -> x7, starting transfers between devices: 5.15 us -> 6.67 us  [shifted(): lax.ppermute(value, name, [(i, (i + step) % count) for i in range(count)])]
    gather x1 -> x2, local copies, waits for them, and re-layouts: 5.34 us -> 5.55 us  [rows_for_half(): return pool[mine].reshape(half_experts, capacity, part)]
  transfers between devices with their start and end apart: 10 -> 12, of which waited for: 8 -> 6; matrix products, arithmetic and copies ran while one was open for 11% -> 17% of each run, Pallas kernels for 0% -> 0%
where the time goes in v2:
time: 250 us; the launch traced here: 249 us
  waiting for transfers between devices  155 us (62%)
  starting transfers between devices  30.9 us (12%)
  matrix products  25.5 us (10%)
  other arithmetic  22.2 us (9%)
  local copies, waits for them, and re-layouts  14.4 us (6%)
    ppermute x7, waiting for transfers between devices, shifted(): lax.ppermute(value, name, [(i, (i + step) % count) for i in range(count)])  62.6 us
    all_to_all x1, waiting for transfers between devices, on_device(): lax.all_to_all(leaving, 'fs', split_axis=0, concat_axis=0, tiled=True)  44.1 us
    all_to_all x1, waiting for transfers between devices, on_device(): lax.all_to_all(both_cast, 'fs', split_axis=0, concat_axis=0, tiled=True)  39.2 us
    dot_general x4, matrix products, hidden_of(): jnp.einsum('enk,ekh->enh', piece, gate_piece, preferred_element_type=jnp....  11.3 us
    dot_general x4, matrix products, hidden_of(): jnp.einsum('enk,ekh->enh', piece, up_piece, preferred_element_type=jnp.fl...  10.2 us
    all_to_all x2, starting transfers between devices, over_half(): lax.all_to_all(outgoing, 'fs', split_axis=0, concat_axis=0, tiled=True, a...  8.7 us
    all_to_all x2, waiting for transfers between devices, over_half(): lax.all_to_all(outgoing, 'fs', split_axis=0, concat_axis=0, tiled=True, a...  8.67 us
    all_to_all x1, starting transfers between devices, on_device(): lax.all_to_all(both_cast, 'fs', split_axis=0, concat_axis=0, tiled=True)  7.44 us
  transfers between devices with their start and end apart: 12, of which 6 were waited for; matrix products, arithmetic and copies ran while one was open for 17% of the time, Pallas kernels for 0%

profile of v2, /device:TPU:0, one launch (start us, length us, event | category | flops | bytes accessed | tf_op | source)
XLA Modules:
  0.0 248.6 jit_solution(2683690963521399215)
XLA Ops:
  0.6 2.9 %fusion.5 = (bf16[8,1,128,512]{3,2,1,0:T(8,128)(2,1)S(1)}, bf16[8,1,128,512]{3,2,1,0:T(8,128)(2,1)S(1)}) fusion(f32[8,128,512]{2,1,0:T(8,128)} %param.9, f32[128]{0:T(128)} %param.8, f32[8,128,512]{2,1,0:T(8,128)} %param.10), kind=kLoop, calls=%fused_computation.32 | loop fusion | flops 2097152 | bytes 6291968 | tf_op jit(solution)/shard_map/stack | solution.py:40
  5.0 7.4 %all-to-all-start = ((bf16[8,2,128,512]{3,2,1,0:T(8,128)(2,1)}), bf16[8,2,128,512]{3,2,1,0:T(8,128)(2,1)S(1)}, u32[]{:S(2)}, u32[]{:S(2)}) async-start(bf16[8,2,128,512]{3,2,1,0:T(8,128)(2,1)} %pad_maximum_fusion.2), calls=%async_computation | async-start | bytes 4194304 | tf_op jit(solution)/shard_map/all_to_all | solution.py:41
  18.8 2.8 %gather_fusion = bf16[512,1024]{1,0:T(8,128)(2,1)} fusion(bf16[256,1024]{1,0:T(8,128)(2,1)S(1)} %multiply_convert_fusion.2, s32[1024]{0:T(1024)S(1)} %pad_clamp_fusion.2), kind=kCustom, calls=%fused_computation | custom fusion | bytes 2099200 | tf_op jit(solution)/shard_map/gather | solution.py:62
  21.5 39.2 %all-to-all-done = bf16[8,2,128,512]{3,2,1,0:T(8,128)(2,1)S(1)} async-done(((bf16[8,2,128,512]{3,2,1,0:T(8,128)(2,1)}), bf16[8,2,128,512]{3,2,1,0:T(8,128)(2,1)S(1)}, u32[]{:S(2)}, u32[]{:S(2)}) %all-to-all-start) | async-done | bytes 2097184 | tf_op jit(solution)/shard_map/all_to_all | solution.py:41
  60.7 4.3 %all-to-all-start.1 = ((bf16[4,128,1024]{2,1,0:T(8,128)(2,1)}), bf16[4,128,1024]{2,1,0:T(8,128)(2,1)}, u32[]{:S(2)}, u32[]{:S(2)}) async-start(bf16[4,128,1024]{2,1,0:T(8,128)(2,1)} %bitcast.117), calls=%async_computation.1 | async-start | bytes 2097152 | tf_op jit(solution)/shard_map/all_to_all | solution.py:66
  66.5 2.7 %convert_element_type.68 = bf16[8,512,128]{2,1,0:T(8,128)(2,1)} convert(f32[8,512,128]{2,1,0:T(8,128)} %param.11) | non-fusion elementwise | flops 524288 | bytes 3145728 | tf_op jit(solution)/shard_map/convert_element_type | solution.py:39
  69.3 8.7 %all-to-all-done.1 = bf16[4,128,1024]{2,1,0:T(8,128)(2,1)} async-done(((bf16[4,128,1024]{2,1,0:T(8,128)(2,1)}), bf16[4,128,1024]{2,1,0:T(8,128)(2,1)}, u32[]{:S(2)}, u32[]{:S(2)}) %all-to-all-start.1) | async-done | bytes 1048608 | tf_op jit(solution)/shard_map/all_to_all | solution.py:66
  77.9 4.2 %all-to-all-start.2 = ((bf16[8,512,128]{2,1,0:T(8,128)(2,1)}), bf16[8,512,128]{2,1,0:T(8,128)(2,1)}, u32[]{:S(2)}, u32[]{:S(2)}) async-start(bf16[8,512,128]{2,1,0:T(8,128)(2,1)} %convert_element_type.68), calls=%async_computation.2 | async-start | bytes 2097152 | tf_op jit(solution)/shard_map/all_to_all | solution.py:76
  82.2 2.8 %collective-permute-start.1 = (bf16[256,1024]{1,0:T(8,128)(2,1)S(1)}, bf16[256,1024]{1,0:T(8,128)(2,1)S(1)}, u32[]{:S(2)}, u32[]{:S(2)}) collective-permute-start(bf16[256,1024]{1,0:T(8,128)(2,1)S(1)} %multiply_convert_fusion.2), channel_id=1, source_target_pairs={{0,8},{2,10},{4,12},{6,14},{8,0},{10,2},{12,4},{14,6},{1,9},{3,11}... | collective-permute-start | bytes 1572872 | tf_op jit(solution)/shard_map/ppermute | solution.py:11
  85.2 45.1 %collective-permute-done.2 = s32[1024]{0:T(1024)S(1)} collective-permute-done((s32[1024]{0:T(1024)S(1)}, s32[1024]{0:T(1024)S(1)}, u32[]{:S(2)}, u32[]{:S(2)}) %collective-permute-start.2) | collective-permute-done | bytes 4128 | tf_op jit(solution)/shard_map/ppermute | solution.py:11
  130.3 2.8 %gather_fusion.1 = bf16[512,1024]{1,0:T(8,128)(2,1)} fusion(bf16[256,1024]{1,0:T(8,128)(2,1)S(1)} %collective-permute-done.1, s32[1024]{0:T(1024)S(1)} %pad_clamp_fusion.1), kind=kCustom, calls=%fused_computation.1 | custom fusion | bytes 2099200 | tf_op jit(solution)/shard_map/gather | solution.py:62
  133.1 4.4 %all-to-all-start.3 = ((bf16[4,128,1024]{2,1,0:T(8,128)(2,1)}), bf16[4,128,1024]{2,1,0:T(8,128)(2,1)}, u32[]{:S(2)}, u32[]{:S(2)}) async-start(bf16[4,128,1024]{2,1,0:T(8,128)(2,1)} %bitcast.116), calls=%async_computation.3 | async-start | bytes 2097152 | tf_op jit(solution)/shard_map/all_to_all | solution.py:66
  141.3 3.3 %fusion.23 = f32[512,512]{1,0:T(8,128)S(1)} fusion(bf16[1,512,1024]{2,1,0:T(8,128)(2,1)} %bitcast.18, s32[]{:T(128)S(6)} %select_n.147, bf16[1,1024,512]{2,1,0:T(8,128)(2,1)S(1)} %bitcast.104, bf16[1,1024,512]{2,1,0:T(8,128)(2,1)S(1)} %bitcast.109), kind=kOutput, calls=%fused_computation.53 | convolution fusion | flops 538968064 | bytes 4194308 | tf_op jit(solution)/shard_map/enk,ekh->enh/dot_general | solution.py:101
  144.6 3.5 %fusion.21 = f32[512,512]{1,0:T(8,128)} fusion(bf16[1,512,1024]{2,1,0:T(8,128)(2,1)} %bitcast.18, s32[]{:T(128)S(6)} %select_n.147, bf16[1,1024,512]{2,1,0:T(8,128)(2,1)S(1)} %bitcast.118, bf16[1,1024,512]{2,1,0:T(8,128)(2,1)S(1)} %bitcast.123), kind=kOutput, calls=%fused_computation.51 | convolution fusion | flops 538968064 | bytes 4194308 | tf_op jit(solution)/shard_map/enk,ekh->enh/dot_general | solution.py:104
  148.1 3.5 %convolution_add_fusion.3 = f32[512,512]{1,0:T(8,128)} fusion(f32[512,512]{1,0:T(8,128)S(1)} %fusion.23, bf16[1,512,1024]{2,1,0:T(8,128)(2,1)} %collective-permute-done.4, s32[]{:T(128)S(6)} %select_n.149, bf16[1,1024,512]{2,1,0:T(8,128)(2,1)S(1)} %bitcast.105, bf16[1,1024,512]{2,1,0:T(8,128)(2,1)S(1)} %bitcast.110), kind=kOutput, calls=%fused_computation.29 | convolution fusion | flops 539230208 | bytes 5242884 | tf_op jit(solution)/shard_map/enk,ekh->enh/dot_general | solution.py:101
  151.5 13.7 %collective-permute-done.3 = bf16[8,1,512,128]{3,2,0,1:T(8,128)(2,1)S(1)} collective-permute-done((bf16[8,1,512,128]{3,2,0,1:T(8,128)(2,1)}, bf16[8,1,512,128]{3,2,0,1:T(8,128)(2,1)S(1)}, u32[]{:S(2)}, u32[]{:S(2)}) %collective-permute-start.3) | collective-permute-done | bytes 1048608 | tf_op jit(solution)/shard_map/ppermute | solution.py:11
  169.2 3.3 %fusion.42 = f32[512,512]{1,0:T(8,128)S(1)} fusion(bf16[512,1024]{1,0:T(8,128)(2,1)} %bitcast.28, s32[]{:T(128)S(6)} %select_n.147, bf16[1,1024,512]{2,1,0:T(8,128)(2,1)S(1)} %bitcast.106, bf16[1,1024,512]{2,1,0:T(8,128)(2,1)S(1)} %bitcast.111), kind=kOutput, calls=%fused_computation.94 | convolution fusion | flops 538968064 | bytes 4194308 | tf_op jit(solution)/shard_map/enk,ekh->enh/dot_general | solution.py:101
  177.8 2.8 %select_bitcast_fusion.3 = (bf16[1,512,512]{2,1,0:T(8,128)(2,1)S(1)}, bf16[1,512,512]{2,1,0:T(8,128)(2,1)S(1)}) fusion(bf16[512,512]{1,0:T(8,128)(2,1)S(1)} %fusion.4, pred[]{:T(512)S(6)} %eq.54, f32[512,512]{1,0:T(8,128)S(1)} %copy-done.11, s32[]{:T(128)S(6)} %select_n.149, bf16[1,1024,512]{2,1,0:T(8,128)(2,1)S(1)} %bitcast.122, ...), kind=kOutput, calls=%fused_computation.61 | convolution fusion | flops 541327360 | bytes 6815749 | tf_op jit(solution)/shard_map/enk,ekh->enh/dot_general | solution.py:104
  182.4 3.8 %collective-permute-done.6 = bf16[1,1024,1024]{2,1,0:T(8,128)(2,1)S(1)} collective-permute-done((bf16[1,1024,1024]{2,1,0:T(8,128)(2,1)S(1)}, bf16[1,1024,1024]{2,1,0:T(8,128)(2,1)S(1)}, u32[]{:S(2)}, u32[]{:S(2)}) %collective-permute-start.6) | collective-permute-done | bytes 2097184 | tf_op jit(solution)/shard_map/ppermute | solution.py:11
  186.2 2.8 %fusion = bf16[1,1024,1024]{2,1,0:T(8,128)(2,1)} fusion(bf16[1,1024,1024]{2,1,0:T(8,128)(2,1)S(1)} %collective-permute-done.6, bf16[1,512,2048]{2,1,0:T(8,128)(2,1)S(1)} %bitcast_dynamic-update-slice_fusion, s32[]{:T(128)S(6)} %select_n.147, bf16[1,512,512]{2,1,0:T(8,128)(2,1)S(1)} %get-tuple-element.25, bf16[1,512,512]{2,1,0:T(8,128)(2,1)S(1)} %get-tuple-element.24), kind=kOutput, calls=%fused_computation.5 | convolution fusion | flops 1081081856 | bytes 6291460 | tf_op jit(solution)/shard_map/enh,ehk->enk/dot_general | solution.py:122
  189.0 3.8 %all-to-all-start.4 = ((bf16[8,128,1024]{2,1,0:T(8,128)(2,1)}), bf16[8,128,1024]{2,1,0:T(8,128)(2,1)S(1)}, u32[]{:S(2)}, u32[]{:S(2)}) async-start(bf16[8,128,1024]{2,1,0:T(8,128)(2,1)} %bitcast.128), calls=%async_computation.4 | async-start | bytes 4194304 | tf_op jit(solution)/shard_map/all_to_all | solution.py:129
  193.1 3.1 %pad_maximum_fusion.1 = bf16[1,2048,512]{2,1,0:T(8,128)(2,1)} fusion(bf16[1,1024,512]{2,1,0:T(8,128)(2,1)} %bitcast.124, bf16[1,1024,512]{2,1,0:T(8,128)(2,1)} %bitcast.119), kind=kLoop, calls=%fused_computation.13 | loop fusion | flops 4194304 | bytes 4194304 | tf_op jit(solution)/shard_map/concatenate | solution.py:86
  197.6 44.1 %all-to-all-done.4 = bf16[8,128,1024]{2,1,0:T(8,128)(2,1)S(1)} async-done(((bf16[8,128,1024]{2,1,0:T(8,128)(2,1)}), bf16[8,128,1024]{2,1,0:T(8,128)(2,1)S(1)}, u32[]{:S(2)}, u32[]{:S(2)}) %all-to-all-start.4) | async-done | bytes 2097184 | tf_op jit(solution)/shard_map/all_to_all | solution.py:129
  245.2 3.5 %multiply_reduce_fusion = bf16[256,1024]{1,0:T(8,128)(2,1)} fusion(f32[256,2,1024]{2,1,0:T(2,128)S(1)} %reshape.253, f32[256,2]{1,0:T(8,128)S(1)} %copy.26), kind=kLoop, calls=%fused_computation.17 | loop fusion | flops 786432 | bytes 2623488 | tf_op jit(solution)/shard_map/reduce_sum | solution.py:133
  (77 shorter events, 29.2 us)
Async XLA Ops:
  5.0 7.4 %copy-start.9 = (s32[256,2]{0,1:T(2,128)S(1)}, s32[256,2]{0,1:T(2,128)}, u32[]{:S(2)}) copy-start(s32[256,2]{0,1:T(2,128)} %param.12) | copy-start | bytes 6148
  5.0 12.2 %copy-start.6 = (bf16[256,2048]{1,0:T(8,128)(2,1)S(1)}, bf16[256,2048]{1,0:T(8,128)(2,1)}, u32[]{:S(2)}) copy-start(bf16[256,2048]{1,0:T(8,128)(2,1)} %param.7) | copy-start | bytes 3145732
  5.0 55.7 %all-to-all-start = ((bf16[8,2,128,512]{3,2,1,0:T(8,128)(2,1)}), bf16[8,2,128,512]{3,2,1,0:T(8,128)(2,1)S(1)}, u32[]{:S(2)}, u32[]{:S(2)}) async-start(bf16[8,2,128,512]{3,2,1,0:T(8,128)(2,1)} %pad_maximum_fusion.2), calls=%async_computation | async-start | bytes 4194304 | tf_op jit(solution)/shard_map/all_to_all | solution.py:41
  60.7 17.2 %all-to-all-start.1 = ((bf16[4,128,1024]{2,1,0:T(8,128)(2,1)}), bf16[4,128,1024]{2,1,0:T(8,128)(2,1)}, u32[]{:S(2)}, u32[]{:S(2)}) async-start(bf16[4,128,1024]{2,1,0:T(8,128)(2,1)} %bitcast.117), calls=%async_computation.1 | async-start | bytes 2097152 | tf_op jit(solution)/shard_map/all_to_all | solution.py:66
  65.0 72.6 %collective-permute-start = (bf16[8,1,2,128,512]{4,3,2,0,1:T(8,128)(2,1)S(1)}, bf16[8,1,2,128,512]{4,3,2,0,1:T(8,128)(2,1)}, u32[]{:S(2)}, u32[]{:S(2)}) collective-permute-start(bf16[8,1,2,128,512]{4,3,2,0,1:T(8,128)(2,1)S(1)} %bitcast.114), channel_id=1, source_target_pairs={{0,16},{16,0},{1,17},{17,1},{2,18},{18,2},{3,19},{19,3},{4,20},{20... | collective-permute-start | bytes 6291464 | tf_op jit(solution)/shard_map/ppermute | solution.py:11
  77.9 55.2 %all-to-all-start.2 = ((bf16[8,512,128]{2,1,0:T(8,128)(2,1)}), bf16[8,512,128]{2,1,0:T(8,128)(2,1)}, u32[]{:S(2)}, u32[]{:S(2)}) async-start(bf16[8,512,128]{2,1,0:T(8,128)(2,1)} %convert_element_type.68), calls=%async_computation.2 | async-start | bytes 2097152 | tf_op jit(solution)/shard_map/all_to_all | solution.py:76
  82.2 48.1 %collective-permute-start.1 = (bf16[256,1024]{1,0:T(8,128)(2,1)S(1)}, bf16[256,1024]{1,0:T(8,128)(2,1)S(1)}, u32[]{:S(2)}, u32[]{:S(2)}) collective-permute-start(bf16[256,1024]{1,0:T(8,128)(2,1)S(1)} %multiply_convert_fusion.2), channel_id=1, source_target_pairs={{0,8},{2,10},{4,12},{6,14},{8,0},{10,2},{12,4},{14,6},{1,9},{3,11}... | collective-permute-start | bytes 1572872 | tf_op jit(solution)/shard_map/ppermute | solution.py:11
  85.0 45.3 %collective-permute-start.2 = (s32[1024]{0:T(1024)S(1)}, s32[1024]{0:T(1024)S(1)}, u32[]{:S(2)}, u32[]{:S(2)}) collective-permute-start(s32[1024]{0:T(1024)S(1)} %scatter_custom_fusion), channel_id=1, source_target_pairs={{0,8},{2,10},{4,12},{6,14},{8,0},{10,2},{12,4},{14,6},{1,9},{3,11}... | collective-permute-start | bytes 12296 | tf_op jit(solution)/shard_map/ppermute | solution.py:11
  133.1 15.0 %collective-permute-start.4 = (bf16[1,512,1024]{2,1,0:T(8,128)(2,1)}, bf16[1,512,1024]{2,1,0:T(8,128)(2,1)}, u32[]{:S(2)}, u32[]{:S(2)}) collective-permute-start(bf16[1,512,1024]{2,1,0:T(8,128)(2,1)} %bitcast.18), channel_id=1, source_target_pairs={{0,1},{1,0},{2,3},{3,2},{4,5},{5,4},{6,7},{7,6},{8,9},{9,8},{10,11... | collective-permute-start | bytes 3145736 | tf_op jit(solution)/shard_map/ppermute | solution.py:11
  133.1 34.5 %all-to-all-start.3 = ((bf16[4,128,1024]{2,1,0:T(8,128)(2,1)}), bf16[4,128,1024]{2,1,0:T(8,128)(2,1)}, u32[]{:S(2)}, u32[]{:S(2)}) async-start(bf16[4,128,1024]{2,1,0:T(8,128)(2,1)} %bitcast.116), calls=%async_computation.3 | async-start | bytes 2097152 | tf_op jit(solution)/shard_map/all_to_all | solution.py:66
  139.4 25.8 %collective-permute-start.3 = (bf16[8,1,512,128]{3,2,0,1:T(8,128)(2,1)}, bf16[8,1,512,128]{3,2,0,1:T(8,128)(2,1)S(1)}, u32[]{:S(2)}, u32[]{:S(2)}) collective-permute-start(bf16[8,1,512,128]{3,2,0,1:T(8,128)(2,1)} %bitcast.19), channel_id=1, source_target_pairs={{0,16},{16,0},{1,17},{17,1},{2,18},{18,2},{3,19},{19,3},{4,20},{20... | collective-permute-start | bytes 3145736 | tf_op jit(solution)/shard_map/ppermute | solution.py:11
  141.3 3.3 %copy-start.2 = (bf16[8,1,1,128,512]{4,3,2,0,1:T(8,128)(2,1)}, bf16[8,1,1,128,512]{4,3,2,0,1:T(8,128)(2,1)S(1)}, u32[]{:S(2)}) copy-start(bf16[8,1,1,128,512]{4,3,2,0,1:T(8,128)(2,1)S(1)} %get-tuple-element.20) | copy-start | bytes 3145732
  141.3 3.3 %copy-start.4 = (bf16[8,1,1,128,512]{4,3,2,0,1:T(8,128)(2,1)}, bf16[8,1,1,128,512]{4,3,2,0,1:T(8,128)(2,1)S(1)}, u32[]{:S(2)}) copy-start(bf16[8,1,1,128,512]{4,3,2,0,1:T(8,128)(2,1)S(1)} %get-tuple-element.29) | copy-start | bytes 3145732
  141.3 33.7 %copy-start = (bf16[8,1,1,128,512]{4,3,2,0,1:T(8,128)(2,1)}, bf16[8,1,1,128,512]{4,3,2,0,1:T(8,128)(2,1)S(1)}, u32[]{:S(2)}) copy-start(bf16[8,1,1,128,512]{4,3,2,0,1:T(8,128)(2,1)S(1)} %get-tuple-element.28) | copy-start | bytes 3145732
  167.6 7.3 %collective-permute-start.5 = (bf16[1,512,1024]{2,1,0:T(8,128)(2,1)}, bf16[1,512,1024]{2,1,0:T(8,128)(2,1)S(1)}, u32[]{:S(2)}, u32[]{:S(2)}) collective-permute-start(bf16[1,512,1024]{2,1,0:T(8,128)(2,1)} %bitcast.29), channel_id=1, source_target_pairs={{0,1},{1,0},{2,3},{3,2},{4,5},{5,4},{6,7},{7,6},{8,9},{9,8},{10,11... | collective-permute-start | bytes 3145736 | tf_op jit(solution)/shard_map/ppermute | solution.py:11
  169.2 17.1 %copy-start.8 = (bf16[1,512,2048]{2,1,0:T(8,128)(2,1)}, bf16[1,512,2048]{2,1,0:T(8,128)(2,1)S(1)}, u32[]{:S(2)}) copy-start(bf16[1,512,2048]{2,1,0:T(8,128)(2,1)S(1)} %bitcast_dynamic-update-slice_fusion) | copy-start | bytes 6291460
  169.2 3.3 %copy-start.3 = (bf16[8,1,1,128,512]{4,3,2,0,1:T(8,128)(2,1)S(1)}, bf16[8,1,1,128,512]{4,3,2,0,1:T(8,128)(2,1)}, u32[]{:S(2)}) copy-start(bf16[8,1,1,128,512]{4,3,2,0,1:T(8,128)(2,1)} %copy-done.2) | copy-start | bytes 3145732
  169.2 3.3 %copy-start.5 = (bf16[8,1,1,128,512]{4,3,2,0,1:T(8,128)(2,1)S(1)}, bf16[8,1,1,128,512]{4,3,2,0,1:T(8,128)(2,1)}, u32[]{:S(2)}) copy-start(bf16[8,1,1,128,512]{4,3,2,0,1:T(8,128)(2,1)} %copy-done.4) | copy-start | bytes 3145732
  176.2 1.5 copy-start.7
  176.3 1.5 copy-start.11
  181.8 4.4 %collective-permute-start.6 = (bf16[1,1024,1024]{2,1,0:T(8,128)(2,1)S(1)}, bf16[1,1024,1024]{2,1,0:T(8,128)(2,1)S(1)}, u32[]{:S(2)}, u32[]{:S(2)}) collective-permute-start(bf16[1,1024,1024]{2,1,0:T(8,128)(2,1)S(1)} %convert_bitcast_fusion), channel_id=1, source_target_pairs={{0,1},{1,0},{2,3},{3,2},{4,5},{5,4},{6,7},{7,6},{8,9},{9,8},{10,11... | collective-permute-start | bytes 6291464 | tf_op jit(solution)/shard_map/ppermute | solution.py:11
  189.0 3.8 %copy-start.10 = (f32[256,2]{0,1:T(2,128)S(1)}, f32[256,2]{0,1:T(2,128)}, u32[]{:S(2)}) copy-start(f32[256,2]{0,1:T(2,128)} %param.13) | copy-start | bytes 6148
  189.0 52.7 %all-to-all-start.4 = ((bf16[8,128,1024]{2,1,0:T(8,128)(2,1)}), bf16[8,128,1024]{2,1,0:T(8,128)(2,1)S(1)}, u32[]{:S(2)}, u32[]{:S(2)}) async-start(bf16[8,128,1024]{2,1,0:T(8,128)(2,1)} %bitcast.128), calls=%async_computation.4 | async-start | bytes 4194304 | tf_op jit(solution)/shard_map/all_to_all | solution.py:129
  193.0 3.1 %copy-start.1 = (bf16[8,1,1,128,512]{4,3,2,0,1:T(8,128)(2,1)S(1)}, bf16[8,1,1,128,512]{4,3,2,0,1:T(8,128)(2,1)}, u32[]{:S(2)}) copy-start(bf16[8,1,1,128,512]{4,3,2,0,1:T(8,128)(2,1)} %copy-done) | copy-start | bytes 3145732

commit v3 on v1

--- a/solution.py
+++ b/solution.py
@@ -115,11 +115,11 @@
     leaving = expert_out.transpose(2, 1, 0, 3, 4).reshape(experts, capacity, part)
     returned = lax.all_to_all(leaving, "fs", split_axis=0, concat_axis=0, tiled=True)
     flat_back = returned.reshape(experts * capacity, part)
-    picked = flat_back[slot_index].reshape(tok_count, 2, part)
     route_share = route_score / jnp.sum(route_score, axis=-1, keepdims=True)
-    mixed = jnp.sum(picked.astype(jnp.float32) * route_share[:, :, None], axis=1).astype(
-        jnp.bfloat16
-    )
+    pick_slots = slot_index.reshape(tok_count, 2)
+    mixed = sum(
+        flat_back[pick_slots[:, k]].astype(jnp.float32) * route_share[:, k, None] for k in range(2)
+    ).astype(jnp.bfloat16)
     return (gate_ready, up_ready, down_ready, mixed)
 
 

time: 275 us -> 271 us (0.985)
    reduce_sum x1 -> x0, other arithmetic: 3.47 us -> none  [on_device(): jnp.sum(picked.astype(jnp.float32) * route_share[:, :, None], axis=1)]
  transfers between devices with their start and end apart: 10 -> 10, of which waited for: 8 -> 8; matrix products, arithmetic and copies ran while one was open for 11% -> 12% of each run, Pallas kernels for 0% -> 0%
where the time goes in v3:
time: 271 us
  waiting for transfers between devices  196 us (72%)
  starting transfers between devices  26.4 us (10%)
  other arithmetic  21 us (8%)
  local copies, waits for them, and re-layouts  14.1 us (5%)
  matrix products  12.6 us (5%)
    ppermute x6, waiting for transfers between devices, shifted(): lax.ppermute(value, name, [(i, (i + step) % count) for i in range(count)])  86.5 us
    all_to_all x1, waiting for transfers between devices, on_device(): lax.all_to_all(leaving, 'fs', split_axis=0, concat_axis=0, tiled=True)  43.7 us
    all_to_all x1, waiting for transfers between devices, on_device(): lax.all_to_all(both_cast, 'fs', split_axis=0, concat_axis=0, tiled=True)  43.4 us
    all_to_all x1, waiting for transfers between devices, on_device(): lax.all_to_all(outgoing, 'fs', split_axis=0, concat_axis=0, tiled=True, a...  21.9 us
    all_to_all x1, starting transfers between devices, on_device(): lax.all_to_all(both_cast, 'fs', split_axis=0, concat_axis=0, tiled=True)  7.44 us
  transfers between devices with their start and end apart: 10, of which 8 were waited for; matrix products, arithmetic and copies ran while one was open for 12% of the time, Pallas kernels for 0%

profile of v3, /device:TPU:0, one launch (start us, length us, event | category | flops | bytes accessed | tf_op | source)
XLA Modules:
  0.0 270.6 jit_solution(13468877579853056695)
XLA Ops:
  0.6 2.9 %fusion.7 = (bf16[8,1,128,512]{3,2,1,0:T(8,128)(2,1)S(1)}, bf16[8,1,128,512]{3,2,1,0:T(8,128)(2,1)S(1)}) fusion(f32[8,128,512]{2,1,0:T(8,128)} %param.9, f32[128]{0:T(128)} %param.8, f32[8,128,512]{2,1,0:T(8,128)} %param.10), kind=kLoop, calls=%fused_computation.28 | loop fusion | flops 2097152 | bytes 6291968 | tf_op jit(solution)/shard_map/stack | solution.py:40
  5.0 7.4 %all-to-all-start = ((bf16[8,2,128,512]{3,2,1,0:T(8,128)(2,1)}), bf16[8,2,128,512]{3,2,1,0:T(8,128)(2,1)S(1)}, u32[]{:S(2)}, u32[]{:S(2)}) async-start(bf16[8,2,128,512]{3,2,1,0:T(8,128)(2,1)} %pad_maximum_fusion.2), calls=%async_computation | async-start | bytes 4194304 | tf_op jit(solution)/shard_map/all_to_all | solution.py:41
  14.6 2.7 %convert_element_type.58 = bf16[8,512,128]{2,1,0:T(8,128)(2,1)} convert(f32[8,512,128]{2,1,0:T(8,128)} %param.11) | non-fusion elementwise | flops 524288 | bytes 3145728 | tf_op jit(solution)/shard_map/convert_element_type | solution.py:39
  17.3 43.4 %all-to-all-done = bf16[8,2,128,512]{3,2,1,0:T(8,128)(2,1)S(1)} async-done(((bf16[8,2,128,512]{3,2,1,0:T(8,128)(2,1)}), bf16[8,2,128,512]{3,2,1,0:T(8,128)(2,1)S(1)}, u32[]{:S(2)}, u32[]{:S(2)}) %all-to-all-start) | async-done | bytes 2097184 | tf_op jit(solution)/shard_map/all_to_all | solution.py:41
  60.7 4.2 %all-to-all-start.1 = ((bf16[8,512,128]{2,1,0:T(8,128)(2,1)}), bf16[8,512,128]{2,1,0:T(8,128)(2,1)}, u32[]{:S(2)}, u32[]{:S(2)}) async-start(bf16[8,512,128]{2,1,0:T(8,128)(2,1)} %convert_element_type.58), calls=%async_computation.1 | async-start | bytes 2097152 | tf_op jit(solution)/shard_map/all_to_all | solution.py:70
  66.7 2.4 scatter_custom_fusion
  69.2 2.9 %collective-permute-start.2 = (s32[1024]{0:T(1024)S(1)}, s32[1024]{0:T(1024)S(1)}, u32[]{:S(2)}, u32[]{:S(2)}) collective-permute-start(s32[1024]{0:T(1024)S(1)} %scatter_custom_fusion), channel_id=1, source_target_pairs={{0,8},{2,10},{4,12},{6,14},{8,0},{10,2},{12,4},{14,6},{1,9},{3,11}... | collective-permute-start | bytes 12296 | tf_op jit(solution)/shard_map/ppermute | solution.py:11
  73.4 30.0 %collective-permute-done.2 = s32[1024]{0:T(1024)S(1)} collective-permute-done((s32[1024]{0:T(1024)S(1)}, s32[1024]{0:T(1024)S(1)}, u32[]{:S(2)}, u32[]{:S(2)}) %collective-permute-start.2) | collective-permute-done | bytes 4128 | tf_op jit(solution)/shard_map/ppermute | solution.py:11
  103.5 9.8 %collective-permute-done.1 = bf16[256,1024]{1,0:T(8,128)(2,1)} collective-permute-done((bf16[256,1024]{1,0:T(8,128)(2,1)}, bf16[256,1024]{1,0:T(8,128)(2,1)}, u32[]{:S(2)}, u32[]{:S(2)}) %collective-permute-start.1) | collective-permute-done | bytes 524320 | tf_op jit(solution)/shard_map/ppermute | solution.py:11
  114.5 5.3 %gather_fusion = bf16[1024,1024]{1,0:T(8,128)(2,1)} fusion(bf16[512,1024]{1,0:T(8,128)(2,1)S(1)} %pad_maximum_fusion.3, s32[1024]{0:T(1024)S(1)} %broadcast_clamp_fusion), kind=kCustom, calls=%fused_computation | custom fusion | bytes 4198400 | tf_op jit(solution)/shard_map/gather | solution.py:67
  119.8 4.6 %all-to-all-start.2 = ((bf16[4,2,128,1024]{3,2,1,0:T(8,128)(2,1)}), bf16[4,2,128,1024]{3,2,1,0:T(8,128)(2,1)}, u32[]{:S(2)}, u32[]{:S(2)}) async-start(bf16[4,2,128,1024]{3,2,1,0:T(8,128)(2,1)} %bitcast.87), calls=%async_computation.2 | async-start | bytes 4194304 | tf_op jit(solution)/shard_map/all_to_all | solution.py:74
  124.5 1.6 collective-permute-start
  126.5 21.9 %all-to-all-done.2 = bf16[4,2,128,1024]{3,2,1,0:T(8,128)(2,1)} async-done(((bf16[4,2,128,1024]{3,2,1,0:T(8,128)(2,1)}), bf16[4,2,128,1024]{3,2,1,0:T(8,128)(2,1)}, u32[]{:S(2)}, u32[]{:S(2)}) %all-to-all-start.2) | async-done | bytes 2097184 | tf_op jit(solution)/shard_map/all_to_all | solution.py:74
  148.4 24.7 %collective-permute-done = bf16[8,1,2,128,512]{4,3,2,0,1:T(8,128)(2,1)} collective-permute-done((bf16[8,1,2,128,512]{4,3,2,0,1:T(8,128)(2,1)S(1)}, bf16[8,1,2,128,512]{4,3,2,0,1:T(8,128)(2,1)}, u32[]{:S(2)}, u32[]{:S(2)}) %collective-permute-start) | collective-permute-done | bytes 2097184 | tf_op jit(solution)/shard_map/ppermute | solution.py:11
  173.1 1.9 broadcast_select_fusion.1
  175.3 17.9 %collective-permute-done.3 = bf16[8,1,512,128]{3,2,0,1:T(8,128)(2,1)} collective-permute-done((bf16[8,1,512,128]{3,2,0,1:T(8,128)(2,1)}, bf16[8,1,512,128]{3,2,0,1:T(8,128)(2,1)}, u32[]{:S(2)}, u32[]{:S(2)}) %collective-permute-start.3) | collective-permute-done | bytes 1048608 | tf_op jit(solution)/shard_map/ppermute | solution.py:11
  193.2 1.7 select_bitcast_fusion
  195.2 3.8 %fusion.18 = f32[1024,512]{1,0:T(8,128)S(1)} fusion(bf16[1024,1024]{1,0:T(8,128)(2,1)} %bitcast.23, s32[]{:T(128)S(6)} %select_n.153, bf16[1,1024,512]{2,1,0:T(8,128)(2,1)S(1)} %bitcast.89, bf16[1,1024,512]{2,1,0:T(8,128)(2,1)S(1)} %bitcast.92), kind=kOutput, calls=%fused_computation.37 | convolution fusion | flops 1075838976 | bytes 6291460 | tf_op jit(solution)/shard_map/enk,ekh->enh/dot_general | solution.py:98
  199.0 3.0 %fusion.11 = f32[1024,512]{1,0:T(8,128)S(1)} fusion(bf16[1024,1024]{1,0:T(8,128)(2,1)} %bitcast.23, s32[]{:T(128)S(6)} %select_n.153, bf16[1,1024,512]{2,1,0:T(8,128)(2,1)S(1)} %bitcast.95, bf16[1,1024,512]{2,1,0:T(8,128)(2,1)S(1)} %bitcast.98), kind=kOutput, calls=%fused_computation.32 | convolution fusion | flops 1075838976 | bytes 6291460 | tf_op jit(solution)/shard_map/enk,ekh->enh/dot_general | solution.py:101
  203.6 1.8 multiply_convert_fusion
  206.7 4.1 %collective-permute-done.5 = bf16[1,1024,1024]{2,1,0:T(8,128)(2,1)S(1)} collective-permute-done((bf16[1,1024,1024]{2,1,0:T(8,128)(2,1)S(1)}, bf16[1,1024,1024]{2,1,0:T(8,128)(2,1)S(1)}, u32[]{:S(2)}, u32[]{:S(2)}) %collective-permute-start.5) | collective-permute-done | bytes 2097184 | tf_op jit(solution)/shard_map/ppermute | solution.py:11
  213.7 5.0 %all-to-all-start.3 = ((bf16[8,128,1024]{2,1,0:T(8,128)(2,1)}), bf16[8,128,1024]{2,1,0:T(8,128)(2,1)S(1)}, u32[]{:S(2)}, u32[]{:S(2)}) async-start(bf16[8,128,1024]{2,1,0:T(8,128)(2,1)} %bitcast.88), calls=%async_computation.3 | async-start | bytes 4194304 | tf_op jit(solution)/shard_map/all_to_all | solution.py:116
  219.0 3.1 %pad_maximum_fusion.1 = bf16[1,2048,512]{2,1,0:T(8,128)(2,1)} fusion(bf16[1,1024,512]{2,1,0:T(8,128)(2,1)} %bitcast.100, bf16[1,1024,512]{2,1,0:T(8,128)(2,1)} %bitcast.97), kind=kLoop, calls=%fused_computation.13 | loop fusion | flops 4194304 | bytes 4194304 | tf_op jit(solution)/shard_map/concatenate | solution.py:84
  223.5 43.7 %all-to-all-done.3 = bf16[8,128,1024]{2,1,0:T(8,128)(2,1)S(1)} async-done(((bf16[8,128,1024]{2,1,0:T(8,128)(2,1)}), bf16[8,128,1024]{2,1,0:T(8,128)(2,1)S(1)}, u32[]{:S(2)}, u32[]{:S(2)}) %all-to-all-start.3) | async-done | bytes 2097184 | tf_op jit(solution)/shard_map/all_to_all | solution.py:116
  (61 shorter events, 19.8 us)
Async XLA Ops:
  5.0 7.4 %copy-start.7 = (s32[256,2]{0,1:T(2,128)S(1)}, s32[256,2]{0,1:T(2,128)}, u32[]{:S(2)}) copy-start(s32[256,2]{0,1:T(2,128)} %param.12) | copy-start | bytes 6148
  5.0 55.7 %all-to-all-start = ((bf16[8,2,128,512]{3,2,1,0:T(8,128)(2,1)}), bf16[8,2,128,512]{3,2,1,0:T(8,128)(2,1)S(1)}, u32[]{:S(2)}, u32[]{:S(2)}) async-start(bf16[8,2,128,512]{3,2,1,0:T(8,128)(2,1)} %pad_maximum_fusion.2), calls=%async_computation | async-start | bytes 4194304 | tf_op jit(solution)/shard_map/all_to_all | solution.py:41
  17.3 54.7 %copy-start.4 = (bf16[256,2048]{1,0:T(8,128)(2,1)S(1)}, bf16[256,2048]{1,0:T(8,128)(2,1)}, u32[]{:S(2)}) copy-start(bf16[256,2048]{1,0:T(8,128)(2,1)} %param.7) | copy-start | bytes 3145732
  60.7 59.1 %all-to-all-start.1 = ((bf16[8,512,128]{2,1,0:T(8,128)(2,1)}), bf16[8,512,128]{2,1,0:T(8,128)(2,1)}, u32[]{:S(2)}, u32[]{:S(2)}) async-start(bf16[8,512,128]{2,1,0:T(8,128)(2,1)} %convert_element_type.58), calls=%async_computation.1 | async-start | bytes 2097152 | tf_op jit(solution)/shard_map/all_to_all | solution.py:70
  69.2 34.3 %collective-permute-start.2 = (s32[1024]{0:T(1024)S(1)}, s32[1024]{0:T(1024)S(1)}, u32[]{:S(2)}, u32[]{:S(2)}) collective-permute-start(s32[1024]{0:T(1024)S(1)} %scatter_custom_fusion), channel_id=1, source_target_pairs={{0,8},{2,10},{4,12},{6,14},{8,0},{10,2},{12,4},{14,6},{1,9},{3,11}... | collective-permute-start | bytes 12296 | tf_op jit(solution)/shard_map/ppermute | solution.py:11
  73.3 39.9 %collective-permute-start.1 = (bf16[256,1024]{1,0:T(8,128)(2,1)}, bf16[256,1024]{1,0:T(8,128)(2,1)}, u32[]{:S(2)}, u32[]{:S(2)}) collective-permute-start(bf16[256,1024]{1,0:T(8,128)(2,1)} %multiply_convert_fusion.3), channel_id=1, source_target_pairs={{0,8},{2,10},{4,12},{6,14},{8,0},{10,2},{12,4},{14,6},{1,9},{3,11}... | collective-permute-start | bytes 1572872 | tf_op jit(solution)/shard_map/ppermute | solution.py:11
  119.8 28.6 %all-to-all-start.2 = ((bf16[4,2,128,1024]{3,2,1,0:T(8,128)(2,1)}), bf16[4,2,128,1024]{3,2,1,0:T(8,128)(2,1)}, u32[]{:S(2)}, u32[]{:S(2)}) async-start(bf16[4,2,128,1024]{3,2,1,0:T(8,128)(2,1)} %bitcast.87), calls=%async_computation.2 | async-start | bytes 4194304 | tf_op jit(solution)/shard_map/all_to_all | solution.py:74
  124.5 48.7 %collective-permute-start = (bf16[8,1,2,128,512]{4,3,2,0,1:T(8,128)(2,1)S(1)}, bf16[8,1,2,128,512]{4,3,2,0,1:T(8,128)(2,1)}, u32[]{:S(2)}, u32[]{:S(2)}) collective-permute-start(bf16[8,1,2,128,512]{4,3,2,0,1:T(8,128)(2,1)S(1)} %bitcast.85), channel_id=1, source_target_pairs={{0,16},{16,0},{1,17},{17,1},{2,18},{18,2},{3,19},{19,3},{4,20},{20... | collective-permute-start | bytes 6291464 | tf_op jit(solution)/shard_map/ppermute | solution.py:11
  126.0 67.2 %collective-permute-start.3 = (bf16[8,1,512,128]{3,2,0,1:T(8,128)(2,1)}, bf16[8,1,512,128]{3,2,0,1:T(8,128)(2,1)}, u32[]{:S(2)}, u32[]{:S(2)}) collective-permute-start(bf16[8,1,512,128]{3,2,0,1:T(8,128)(2,1)} %bitcast.20), channel_id=1, source_target_pairs={{0,16},{16,0},{1,17},{17,1},{2,18},{18,2},{3,19},{19,3},{4,20},{20... | collective-permute-start | bytes 3145736 | tf_op jit(solution)/shard_map/ppermute | solution.py:11
  148.4 53.6 %collective-permute-start.4 = (bf16[1,1024,1024]{2,1,0:T(8,128)(2,1)}, bf16[1,1024,1024]{2,1,0:T(8,128)(2,1)S(1)}, u32[]{:S(2)}, u32[]{:S(2)}) collective-permute-start(bf16[1,1024,1024]{2,1,0:T(8,128)(2,1)} %bitcast.25), channel_id=1, source_target_pairs={{0,1},{1,0},{2,3},{3,2},{4,5},{5,4},{6,7},{7,6},{8,9},{9,8},{10,11... | collective-permute-start | bytes 6291464 | tf_op jit(solution)/shard_map/ppermute | solution.py:11
  175.3 26.8 %copy-start = (bf16[8,1,1,128,512]{4,3,2,0,1:T(8,128)(2,1)}, bf16[8,1,1,128,512]{4,3,2,0,1:T(8,128)(2,1)S(1)}, u32[]{:S(2)}) copy-start(bf16[8,1,1,128,512]{4,3,2,0,1:T(8,128)(2,1)S(1)} %get-tuple-element.30) | copy-start | bytes 3145732
  175.3 28.3 %copy-start.2 = (bf16[8,1,1,128,512]{4,3,2,0,1:T(8,128)(2,1)}, bf16[8,1,1,128,512]{4,3,2,0,1:T(8,128)(2,1)S(1)}, u32[]{:S(2)}) copy-start(bf16[8,1,1,128,512]{4,3,2,0,1:T(8,128)(2,1)S(1)} %get-tuple-element.18) | copy-start | bytes 3145732
  175.3 28.3 %copy-start.3 = (bf16[8,1,1,128,512]{4,3,2,0,1:T(8,128)(2,1)}, bf16[8,1,1,128,512]{4,3,2,0,1:T(8,128)(2,1)S(1)}, u32[]{:S(2)}) copy-start(bf16[8,1,1,128,512]{4,3,2,0,1:T(8,128)(2,1)S(1)} %get-tuple-element.31) | copy-start | bytes 3145732
  195.2 15.7 %copy-start.5 = (bf16[1,512,2048]{2,1,0:T(8,128)(2,1)}, bf16[1,512,2048]{2,1,0:T(8,128)(2,1)S(1)}, u32[]{:S(2)}) copy-start(bf16[1,512,2048]{2,1,0:T(8,128)(2,1)S(1)} %bitcast_dynamic-update-slice_fusion) | copy-start | bytes 6291460
  206.6 4.2 %collective-permute-start.5 = (bf16[1,1024,1024]{2,1,0:T(8,128)(2,1)S(1)}, bf16[1,1024,1024]{2,1,0:T(8,128)(2,1)S(1)}, u32[]{:S(2)}, u32[]{:S(2)}) collective-permute-start(bf16[1,1024,1024]{2,1,0:T(8,128)(2,1)S(1)} %convert_bitcast_fusion), channel_id=1, source_target_pairs={{0,1},{1,0},{2,3},{3,2},{4,5},{5,4},{6,7},{7,6},{8,9},{9,8},{10,11... | collective-permute-start | bytes 6291464 | tf_op jit(solution)/shard_map/ppermute | solution.py:11
  213.7 5.0 %copy-start.6 = (f32[256,2]{0,1:T(2,128)S(1)}, f32[256,2]{0,1:T(2,128)}, u32[]{:S(2)}) copy-start(f32[256,2]{0,1:T(2,128)} %param.13) | copy-start | bytes 6148
  213.7 53.5 %all-to-all-start.3 = ((bf16[8,128,1024]{2,1,0:T(8,128)(2,1)}), bf16[8,128,1024]{2,1,0:T(8,128)(2,1)S(1)}, u32[]{:S(2)}, u32[]{:S(2)}) async-start(bf16[8,128,1024]{2,1,0:T(8,128)(2,1)} %bitcast.88), calls=%async_computation.3 | async-start | bytes 4194304 | tf_op jit(solution)/shard_map/all_to_all | solution.py:116
  218.9 3.1 %copy-start.1 = (bf16[8,1,1,128,512]{4,3,2,0,1:T(8,128)(2,1)S(1)}, bf16[8,1,1,128,512]{4,3,2,0,1:T(8,128)(2,1)}, u32[]{:S(2)}) copy-start(bf16[8,1,1,128,512]{4,3,2,0,1:T(8,128)(2,1)} %copy-done) | copy-start | bytes 3145732
